TPU v7x, 256 devices: a whole 4x4x8 slice. The times are simulated.
256 devices in a mesh: sp: 32 (over z, x), tp: 8 (over y, core).
Axes of the slice: x: 4, y: 4, z: 8, core: 2. Of those that a mesh axis runs over, the one named last changes fastest.
Arguments:
- tokens: bfloat16 [32768, 2048], P('sp', 'tp'), may hold values from -70 to 70
- w_query: bfloat16 [2048, 1024], P(None, 'tp'), may hold values from -0.125 to 0.125
- w_key: bfloat16 [2048, 1024], P(None, 'tp'), may hold values from -0.125 to 0.125
- w_value: bfloat16 [2048, 1024], P(None, 'tp'), may hold values from -0.125 to 0.125
- w_delta_gate: bfloat16 [2048, 1024], P(None, 'tp'), may hold values from -0.125 to 0.125
- w_glu_value: bfloat16 [2048, 1024], P(None, 'tp'), may hold values from -0.125 to 0.125
- w_glu_gate: bfloat16 [2048, 1024], P(None, 'tp'), may hold values from -0.125 to 0.125
- w_conv_gate: bfloat16 [2048, 1024], P(None, 'tp'), may hold values from -0.125 to 0.125
- w_beta: bfloat16 [2048, 8], replicated, may hold values from -0.125 to 0.125
- w_decay: bfloat16 [2048, 8], replicated, may hold values from -0.125 to 0.125
- decay_log: float32 [8], replicated, may hold values from -12 to -3
- head_gain: float32 [128], replicated, may hold values from 0.1 to 1.9
- conv_taps: bfloat16 [31, 1024], P(None, 'tp'), may hold values from -2.5 to 2.5
- ln_gain: float32 [1024], P('tp'), may hold values from 0.1 to 1.9
- ln_shift: float32 [1024], P('tp'), may hold values from -3 to 3
- out_delta: bfloat16 [1024, 2048], P('tp'), may hold values from -0.125 to 0.125
- out_conv: bfloat16 [1024, 2048], P('tp'), may hold values from -0.125 to 0.125
Outputs:
- mixed_out: bfloat16 [32768, 2048], P(('sp', 'tp'))
All inputs are finite; a program needn't handle non-finite values.
Results may differ from a plain program's by a relative error of at most 0.024.
Values may be sent and summed in bfloat16 or wider, within the bound.
A program may use at most 64 MiB of HBM per device.

v0:
```python
import jax
import jax.numpy as jnp
from jax import lax
from jax.sharding import Mesh
from jax.sharding import PartitionSpec as P

SPAN = 64
SP = ("sp_0", "sp_1")
SP_TP = ("sp_0", "sp_1", "tp")


TINY_NORM = 1e-06
TINY_VAR = 1e-05


def filled_with(shard, identity):
    return jnp.broadcast_to(jnp.asarray(identity, shard.dtype), shard.shape)


def prefix_by_axis(shard, axes, combine, identity):
    before = start = filled_with(shard, identity)
    so_far = shard
    for axis in reversed(axes):
        count, mine = (lax.axis_size(axis), lax.axis_index(axis))
        pieces = lax.all_gather(so_far, axis)
        inside, so_far = (start, start)
        for k in range(count):
            passed = k < mine
            so_far = combine(so_far, pieces[k])
            inside = jnp.where(passed, so_far, inside)
        before = combine(inside, before)
    return before


def shifted(block, axis, distance):
    devices = range(lax.axis_size(axis))
    route = [(i - distance, i) for i in devices if i - distance in devices]
    return lax.ppermute(block, axis, route)


def sent_to_all(shard, axis):
    count = lax.axis_size(axis)
    return lax.all_to_all(
        jnp.broadcast_to(shard[None], (count, *shard.shape)), axis, 0, 0, tiled=True
    )


def over_copies(shard, axis):
    return sent_to_all(shard, axis).sum(axis=0)


def packed_total(arrays, axis):
    ends = [0]
    for a in arrays:
        ends.append(ends[-1] + a.size)
    so_far = over_copies(jnp.concatenate([a.ravel() for a in arrays]), axis)
    return tuple((so_far[b:e].reshape(a.shape) for a, b, e in zip(arrays, ends, ends[1:])))


def block_terms(query, keys, values, strength, log_decay):
    log_sum = jnp.cumsum(log_decay, axis=-1)
    offsets = jnp.arange(SPAN)
    causal = offsets[:, None] >= offsets[None, :]
    strict = offsets[:, None] > offsets[None, :]
    spread = log_sum[..., :, None] - log_sum[..., None, :]
    damping = jnp.where(causal, jnp.exp(jnp.where(causal, spread, 0.0)), 0.0)
    scaled_keys = keys * strength[..., None]
    lower = jnp.where(strict, jnp.einsum("hnid,hnjd->hnij", scaled_keys, keys) * damping, 0.0)
    identity = jnp.eye(SPAN, dtype=jnp.float32)
    right = jnp.concatenate(
        [values * strength[..., None], scaled_keys * jnp.exp(log_sum)[..., None]], axis=-1
    )
    solved = jax.scipy.linalg.solve_triangular(
        identity + lower, right, lower=True, unit_diagonal=True
    )
    width = values.shape[-1]
    scores = jnp.einsum("hnid,hnjd->hnij", query, keys) * damping
    return (log_sum, solved[..., :width], solved[..., width:], scores)


def local(
    tokens,
    w_query,
    w_key,
    w_value,
    w_delta_gate,
    w_glu_value,
    w_glu_gate,
    w_conv_gate,
    w_beta,
    w_decay,
    decay_log,
    head_gain,
    conv_taps,
    ln_gain,
    ln_shift,
    out_delta,
    out_conv,
):
    rows_here = tokens.shape[0]
    tp_size = lax.axis_size("tp")
    width_all = tokens.shape[1] * tp_size
    weights = (
        w_query,
        w_key,
        w_value,
        w_delta_gate,
        w_glu_value,
        w_glu_gate,
        w_conv_gate,
        w_beta,
        w_decay,
    )
    piece = lax.all_gather(tokens, "tp", axis=1, tiled=True)
    totals = tuple(
        (jnp.dot(piece, weight, preferred_element_type=jnp.float32) for weight in weights)
    )
    squares = jnp.sum(jnp.square(piece.astype(jnp.float32)), axis=1)
    sums, squares = (totals, squares)
    inv_rms = lax.rsqrt(squares / width_all + TINY_NORM)[:, None]
    scaled = [summed * inv_rms for summed in sums]
    query_raw, key_raw, value_raw, delta_gate_raw, glu_value_raw, glu_gate_raw, conv_gate_raw = [
        item.astype(jnp.bfloat16) for item in scaled[:7]
    ]
    head_size = head_gain.shape[0]
    heads_here = w_query.shape[1] // head_size
    first_head = lax.axis_index("tp") * heads_here
    strength = jax.nn.sigmoid(lax.dynamic_slice_in_dim(scaled[7], first_head, heads_here, 1))
    rates = jnp.exp(lax.dynamic_slice_in_dim(decay_log, first_head, heads_here, 0))
    log_decay = -rates[None, :] * jax.nn.softplus(
        lax.dynamic_slice_in_dim(scaled[8], first_head, heads_here, 1)
    )
    blocks = rows_here // SPAN

    def to_blocks(raw):
        return jnp.transpose(raw.reshape(blocks, SPAN, heads_here, head_size), (2, 0, 1, 3))

    def unit_rows(array):
        return array * lax.rsqrt(jnp.sum(array * array, axis=-1, keepdims=True) + TINY_NORM)

    query = unit_rows(to_blocks(query_raw.astype(jnp.float32))) * head_size ** (-0.5)
    keys = unit_rows(to_blocks(key_raw.astype(jnp.float32)))
    values = to_blocks(value_raw.astype(jnp.float32))
    strength_blocks = jnp.transpose(strength.reshape(blocks, SPAN, heads_here), (2, 0, 1))
    decay_blocks = jnp.transpose(log_decay.reshape(blocks, SPAN, heads_here), (2, 0, 1))
    log_sum, corrected, key_terms, scores = block_terms(
        query, keys, values, strength_blocks, decay_blocks
    )

    def advance(memory, inputs):
        query_block, keys_block, corrected_block, terms_block, scores_block, log_block = inputs
        extended = jnp.concatenate([jnp.zeros_like(corrected_block), corrected_block], axis=-1)
        fresh = extended - jnp.einsum("hcd,hde->hce", terms_block, memory)
        output = jnp.einsum("hcd,hde->hce", query_block * jnp.exp(log_block)[..., None], memory)
        output = output + jnp.einsum("hcs,hse->hce", scores_block, fresh)
        tail_log = log_block[:, -1:]
        weighted = keys_block * jnp.exp(tail_log - log_block)[..., None]
        memory = memory * jnp.exp(tail_log)[..., None] + jnp.einsum("hcd,hce->hde", weighted, fresh)
        return (memory, output)

    start_state = jnp.concatenate(
        [
            jnp.broadcast_to(
                jnp.eye(head_size, dtype=jnp.float32), (heads_here, head_size, head_size)
            ),
            jnp.zeros((heads_here, head_size, head_size), jnp.float32),
        ],
        axis=-1,
    )
    sequence_inputs = tuple(
        (jnp.moveaxis(item, 1, 0) for item in (query, keys, corrected, key_terms, scores, log_sum))
    )
    final, outputs = lax.scan(advance, start_state, sequence_inputs)
    outputs = jnp.moveaxis(outputs, 0, 1).reshape(heads_here, rows_here, 2 * head_size)

    def compose(earlier, later):
        moved = jnp.einsum("hij,hjk->hik", later[..., :head_size], earlier)
        return moved + jnp.concatenate(
            [jnp.zeros_like(later[..., :head_size]), later[..., head_size:]], axis=-1
        )

    prefix = prefix_by_axis(final, SP, compose, start_state)
    carried = prefix[..., head_size:]
    result = outputs[..., head_size:] + jnp.einsum(
        "htd,hde->hte", outputs[..., :head_size], carried
    )
    result = jnp.transpose(result, (1, 0, 2))
    result = (
        result
        * lax.rsqrt(jnp.mean(result * result, axis=-1, keepdims=True) + TINY_NORM)
        * head_gain
    )
    delta_mixed = (
        result.reshape(rows_here, heads_here * head_size)
        * jax.nn.silu(delta_gate_raw.astype(jnp.float32))
    ).astype(jnp.bfloat16)
    kernel = conv_taps.shape[0]
    channels = conv_taps.shape[1]
    gated_units = (
        glu_value_raw.astype(jnp.float32) * jax.nn.sigmoid(glu_gate_raw.astype(jnp.float32))
    ).astype(jnp.bfloat16)
    before = shifted(gated_units[rows_here - (kernel - 1) :], SP, 1)
    padded = jnp.concatenate([before, gated_units], axis=0)
    filtered = jnp.zeros((rows_here, channels), jnp.float32)
    for offset in range(kernel):
        filtered = filtered + padded[offset : offset + rows_here].astype(jnp.float32) * conv_taps[
            offset
        ].astype(jnp.float32)
    first_sum = jnp.sum(filtered, axis=1)
    second_sum = jnp.sum(filtered * filtered, axis=1)
    first_sum, second_sum = packed_total((first_sum, second_sum), "tp")
    channels_all = channels * tp_size
    center = first_sum / channels_all
    variance = jnp.maximum(second_sum / channels_all - center * center, 0.0)
    normed = (filtered - center[:, None]) * lax.rsqrt(variance + TINY_VAR)[
        :, None
    ] * ln_gain + ln_shift
    conv_mixed = (jax.nn.silu(normed) * jax.nn.silu(conv_gate_raw.astype(jnp.float32))).astype(
        jnp.bfloat16
    )
    summed = jnp.dot(delta_mixed, out_delta, preferred_element_type=jnp.float32)
    return lax.psum_scatter(
        (summed + jnp.dot(conv_mixed, out_conv, preferred_element_type=jnp.float32)).astype(
            jnp.bfloat16
        ),
        "tp",
        scatter_dimension=0,
        tiled=True,
    )


def solution(mesh):
    finer = Mesh(mesh.devices.reshape(8, 4, mesh.shape["tp"]), ("sp_0", "sp_1", "tp"))
    placed = (
        P(SP, "tp"),
        P(None, "tp"),
        P(None, "tp"),
        P(None, "tp"),
        P(None, "tp"),
        P(None, "tp"),
        P(None, "tp"),
        P(None, "tp"),
        P(),
        P(),
        P(),
        P(),
        P(None, "tp"),
        P("tp"),
        P("tp"),
        P("tp", None),
        P("tp", None),
    )
    return jax.shard_map(
        local, mesh=finer, in_specs=placed, out_specs=P(SP_TP, None), check_vma=False
    )
```

profile of v0, /device:TPU:1, one launch (start us, length us, event | category | flops | bytes accessed | tf_op | source)
XLA Modules:
  0.0 363.5 jit_solution(16131292923218178079)
XLA Ops:
  7.3 1.2 dynamic_slice.30
  9.4 1.7 bitcast_convert_fusion.30
  11.1 40.4 %all-gather.5.cloned.1.call-done = bf16[1024,2048]{1,0:T(8,128)(2,1)} async-done(((bf16[1024,256]{1,0:T(8,128)(2,1)}), bf16[1024,2048]{1,0:T(8,128)(2,1)}) %all-gather.5.cloned.1.call-update) | async-done | bytes 4194320 | tf_op jit(solution)/shard_map/all_gather | solution.py:114
  51.5 3.2 multiply_reduce_fusion
  54.9 1.2 fusion.198
  56.1 1.2 fusion.197
  57.8 3.5 multiply_reduce_fusion.4
  62.1 78.6 %custom-call.4 = f32[16,1,64,64]{2,3,1,0:T(8,128)S(1)} custom-call(f32[16,1,64,64]{3,2,1,0:T(8,128)S(1)} %fusion.30), custom_call_target="InvertDiagBlocksLowerTriangular" | custom-call | tf_op jit(solution)/shard_map/jit(_solve_triangular)/vmap()/triangular_solve | solution.py:73
  140.7 3.5 fusion.34
  144.8 1.1 convolution_bitcast_fusion.2
  146.6 1.3 multiply_reduce_fusion.3
  148.0 1.2 fusion.25
  149.2 1.0 multiply_multiply_fusion
  150.3 84.6 %while.12 = (s32[]{:T(128)}, f32[1,128,256]{2,1,0:T(8,128)S(1)}, f32[16,1,64,256]{3,2,1,0:T(8,128)}, f32[16,1,64]{2,1,0:T(1,128)}, f32[16,1,64,128]{3,2,1,0:T(8,...) while((s32[]{:T(128)}, f32[1,128,256]{2,1,0:T(8,128)S(1)}, ...), condition=%wide.region_5.6_spmd, body=%wide.region_4.5_spmd.sunk | while | flops 14811202 | bytes 1019293 | solution.py:173
  152.3 1.2 exponential_bitcast_fusion.3
  154.2 1.5 fusion.250
  157.6 1.3 exponential_bitcast_fusion.3
  159.5 1.5 fusion.250
  162.9 1.3 exponential_bitcast_fusion.3
  164.8 1.5 fusion.250
  168.1 1.2 exponential_bitcast_fusion.3
  170.0 1.5 fusion.250
  173.4 1.3 exponential_bitcast_fusion.3
  175.4 1.5 fusion.250
  178.7 1.2 exponential_bitcast_fusion.3
  180.6 1.5 fusion.250
  183.9 1.2 exponential_bitcast_fusion.3
  185.8 1.5 fusion.250
  189.2 1.3 exponential_bitcast_fusion.3
  191.2 1.5 fusion.250
  194.6 1.3 exponential_bitcast_fusion.3
  196.5 1.5 fusion.250
  199.8 1.2 exponential_bitcast_fusion.3
  201.7 1.5 fusion.250
  205.0 1.2 exponential_bitcast_fusion.3
  206.9 1.5 fusion.250
  210.3 1.3 exponential_bitcast_fusion.3
  212.2 1.5 fusion.250
  215.6 1.2 exponential_bitcast_fusion.3
  217.4 1.5 fusion.250
  220.8 1.3 exponential_bitcast_fusion.3
  222.8 1.5 fusion.250
  226.2 1.3 exponential_bitcast_fusion.3
  228.1 1.5 fusion.250
  231.6 1.3 exponential_bitcast_fusion.3
  233.5 1.5 fusion.250
  235.0 11.1 %all-gather = f32[4,128,256]{2,1,0:T(8,128)S(1)} all-gather(f32[1,128,256]{2,1,0:T(8,128)S(1)} %get-tuple-element.54), channel_id=2, replica_groups=mesh['sp_0'=8,'sp_1'=4,'tp'=8] {'sp_1'}, dimensions={0}, use_global_device_ids=true | all-gather | bytes 655360 | tf_op jit(solution)/shard_map/all_gather | solution.py:25
  247.4 3.6 fusion.48
  251.3 1.2 fusion.42
  252.6 2.1 collective-permute-start
  255.7 2.7 fusion.188
  259.1 8.5 %all-to-all-start = ((f32[8,1,2048]{2,1,0:T(1,128)}), f32[8,1,2048]{2,1,0:T(1,128)S(1)}, u32[]{:S(2)}, u32[]{:S(2)}) async-start(f32[8,1,2048]{2,1,0:T(1,128)} %broadcast_in_dim.36), calls=%async_computation | async-start | bytes 131072 | tf_op jit(solution)/shard_map/all_to_all | solution.py:43
  267.8 4.7 %all-to-all-done = f32[8,1,2048]{2,1,0:T(1,128)S(1)} async-done(((f32[8,1,2048]{2,1,0:T(1,128)}), f32[8,1,2048]{2,1,0:T(1,128)S(1)}, u32[]{:S(2)}, u32[]{:S(2)}) %all-to-all-start) | async-done | bytes 65568 | tf_op jit(solution)/shard_map/all_to_all | solution.py:43
  272.5 11.0 %all-gather.7.cloned.1.call-done = f32[8,128,256]{2,1,0:T(8,128)} async-done(((f32[1,128,256]{2,1,0:T(8,128)}), f32[8,128,256]{2,1,0:T(8,128)}) %all-gather.7.cloned.1.call-update) | async-done | bytes 1048592 | tf_op jit(solution)/shard_map/all_gather | solution.py:25
  283.6 1.1 fusion.191
  285.7 1.0 fusion.54
  288.6 1.0 fusion.57
  289.6 1.0 fusion.58
  290.6 1.0 fusion.59
  291.6 1.8 convolution_bitcast_fusion.4
  293.4 1.2 multiply_reduce_fusion.2
  294.7 9.9 %fusion.81 = f32[1024,2048]{1,0:T(8,128)} fusion(bf16[128,2048]{1,0:T(8,128)(2,1)S(1)} %copy-done, f32[1,1024,128]{2,1,0:T(8,128)S(1)} %get-tuple-element.168, bf16[1024,2048]{1,0:T(8,128)(2,1)} %all-gather.5.cloned.1.call-done, bf16[2048,128]{1,0:T(8,128)(2,1)S(1)} %copy-done.8, f32[128]{0:T(128)S(1)} %copy-done.44, f32[1024]{0:T(1024)S(1)} %add_rsqrt_fusion, ...), kind=kOutput, calls=%fused_computation.153 | convolution fusion | flops 1075183616 | bytes 14164480 | tf_op jit(solution)/shard_map/dot_general | solution.py:221
  304.7 11.0 %add_convert_fusion = bf16[1024,2048]{1,0:T(8,128)(2,1)} fusion(f32[1024,2048]{1,0:T(8,128)} %fusion.81, bf16[128,2048]{1,0:T(8,128)(2,1)S(1)} %copy-done.6, bf16[1024,2048]{1,0:T(8,128)(2,1)} %all-gather.5.cloned.1.call-done, bf16[2048,128]{1,0:T(8,128)(2,1)S(1)} %copy-done.7, f32[1024,128]{1,0:T(8,128)S(1)} %get-tuple-element.113, f32[128]{0:T(128)S(1)} %copy-done.42, ...), kind=kOutput, calls=%fused_computation.32 | convolution fusion | flops 1080164352 | bytes 18363392 | tf_op jit(solution)/shard_map/dot_general | solution.py:223
  315.7 41.4 %reduce-scatter.2.cloned.1.call-done = bf16[128,2048]{1,0:T(8,128)(2,1)} async-done(((bf16[1024,2048]{1,0:T(8,128)(2,1)}), bf16[128,2048]{1,0:T(8,128)(2,1)}) %reduce-scatter.2.cloned.1.call-update) | async-done | bytes 524304 | tf_op jit(solution)/shard_map/reduce_scatter | solution.py:222
  (237 shorter events, 40.0 us)
Async XLA Ops:
  6.5 288.1 %copy-start = (bf16[128,2048]{1,0:T(8,128)(2,1)S(1)}, bf16[128,2048]{1,0:T(8,128)(2,1)}, u32[]{:S(2)}) copy-start(bf16[128,2048]{1,0:T(8,128)(2,1)} %param.34) | copy-start | bytes 1572868
  6.5 48.2 %copy-start.18 = (bf16[2048,8]{0,1:T(8,128)(2,1)S(1)}, bf16[2048,8]{0,1:T(8,128)(2,1)}, u32[]{:S(2)}) copy-start(bf16[2048,8]{0,1:T(8,128)(2,1)} %param.27) | copy-start | bytes 98308
  6.5 44.9 %all-gather.5.cloned.1.call-start = ((), (), s32[]{:S(2)}) async-start(), calls=%async_computation.2 | async-start | bytes 4718592 | tf_op jit(solution)/shard_map/all_gather | solution.py:114
  7.3 276.3 %all-gather.7.cloned.1.call-start = ((), (), s32[]{:S(2)}) async-start(), calls=%async_computation.4 | async-start | bytes 1179648 | tf_op jit(solution)/shard_map/all_gather | solution.py:25
  9.3 52.1 %copy-start.21 = (pred[64,64]{1,0:T(8,128)(4,1)}, pred[64,64]{1,0:T(8,128)(4,1)S(1)}, u32[]{:S(2)}) copy-start(pred[64,64]{1,0:T(8,128)(4,1)S(1)} %get-tuple-element.169) | copy-start | bytes 12292
  51.5 3.4 copy-start.1
  51.5 4.6 %copy-start.19 = (bf16[2048,8]{0,1:T(8,128)(2,1)S(1)}, bf16[2048,8]{0,1:T(8,128)(2,1)}, u32[]{:S(2)}) copy-start(bf16[2048,8]{0,1:T(8,128)(2,1)} %param.28) | copy-start | bytes 98308
  54.9 85.8 %copy-start.10 = (f32[1024]{0:T(1024)}, f32[1024]{0:T(1024)S(1)}, u32[]{:S(2)}) copy-start(f32[1024]{0:T(1024)S(1)} %add_rsqrt_fusion.3) | copy-start | bytes 12292
  54.9 2.8 copy-start.45
  57.7 3.6 copy-start.15
  61.4 83.0 %copy-start.13 = (f32[16,64]{1,0:T(8,128)}, f32[16,64]{1,0:T(8,128)S(1)}, u32[]{:S(2)}) copy-start(f32[16,64]{1,0:T(8,128)S(1)} %rsqrt.42) | copy-start | bytes 12292
  144.3 2.2 copy-start.2
  144.3 2.2 copy-start.11
  144.3 2.3 copy-start.46
  145.9 2.1 copy-start.14
  145.9 2.1 copy-start.16
  145.9 2.1 copy-start.22
  148.0 1.2 copy-start.17
  150.3 97.1 %copy-start.12 = (f32[1024]{0:T(1024)S(1)}, f32[1024]{0:T(1024)}, u32[]{:S(2)}) copy-start(f32[1024]{0:T(1024)} %copy-done.10) | copy-start | bytes 12292
  150.3 97.1 %copy-start.47 = (bf16[2048,128]{1,0:T(8,128)(2,1)S(1)}, bf16[2048,128]{1,0:T(8,128)(2,1)}, u32[]{:S(2)}) copy-start(bf16[2048,128]{1,0:T(8,128)(2,1)} %param.25) | copy-start | bytes 1572868
  247.4 3.6 copy-start.3
  247.4 3.6 copy-start.5
  251.1 3.7 %copy-start.20 = (bf16[31,128]{1,0:T(8,128)(2,1)S(1)}, bf16[31,128]{1,0:T(8,128)(2,1)}, u32[]{:S(2)}) copy-start(bf16[31,128]{1,0:T(8,128)(2,1)} %param.31) | copy-start | bytes 23812
  251.1 4.4 %copy-start.23 = (f32[128]{0:T(128)S(1)}, f32[128]{0:T(128)}, u32[]{:S(2)}) copy-start(f32[128]{0:T(128)} %get-tuple-element.130) | copy-start | bytes 1540
  251.1 4.4 %copy-start.24 = (f32[128]{0:T(128)S(1)}, f32[128]{0:T(128)}, u32[]{:S(2)}) copy-start(f32[128]{0:T(128)} %get-tuple-element.131) | copy-start | bytes 1540
  251.1 4.4 %copy-start.25 = (f32[128]{0:T(128)S(1)}, f32[128]{0:T(128)}, u32[]{:S(2)}) copy-start(f32[128]{0:T(128)} %get-tuple-element.132) | copy-start | bytes 1540
  251.1 4.4 %copy-start.26 = (f32[128]{0:T(128)S(1)}, f32[128]{0:T(128)}, u32[]{:S(2)}) copy-start(f32[128]{0:T(128)} %get-tuple-element.133) | copy-start | bytes 1540
  251.1 4.4 %copy-start.27 = (f32[128]{0:T(128)S(1)}, f32[128]{0:T(128)}, u32[]{:S(2)}) copy-start(f32[128]{0:T(128)} %get-tuple-element.134) | copy-start | bytes 1540
  251.1 4.4 %copy-start.28 = (f32[128]{0:T(128)S(1)}, f32[128]{0:T(128)}, u32[]{:S(2)}) copy-start(f32[128]{0:T(128)} %get-tuple-element.135) | copy-start | bytes 1540
  251.1 4.4 %copy-start.29 = (f32[128]{0:T(128)S(1)}, f32[128]{0:T(128)}, u32[]{:S(2)}) copy-start(f32[128]{0:T(128)} %get-tuple-element.136) | copy-start | bytes 1540
  251.2 4.4 %copy-start.30 = (f32[128]{0:T(128)S(1)}, f32[128]{0:T(128)}, u32[]{:S(2)}) copy-start(f32[128]{0:T(128)} %get-tuple-element.137) | copy-start | bytes 1540
  251.2 4.4 %copy-start.31 = (f32[128]{0:T(128)S(1)}, f32[128]{0:T(128)}, u32[]{:S(2)}) copy-start(f32[128]{0:T(128)} %get-tuple-element.138) | copy-start | bytes 1540
  251.2 4.4 %copy-start.32 = (f32[128]{0:T(128)S(1)}, f32[128]{0:T(128)}, u32[]{:S(2)}) copy-start(f32[128]{0:T(128)} %get-tuple-element.139) | copy-start | bytes 1540
  251.2 4.4 %copy-start.33 = (f32[128]{0:T(128)S(1)}, f32[128]{0:T(128)}, u32[]{:S(2)}) copy-start(f32[128]{0:T(128)} %get-tuple-element.140) | copy-start | bytes 1540
  251.2 4.4 %copy-start.34 = (f32[128]{0:T(128)S(1)}, f32[128]{0:T(128)}, u32[]{:S(2)}) copy-start(f32[128]{0:T(128)} %get-tuple-element.141) | copy-start | bytes 1540
  251.2 4.4 %copy-start.35 = (f32[128]{0:T(128)S(1)}, f32[128]{0:T(128)}, u32[]{:S(2)}) copy-start(f32[128]{0:T(128)} %get-tuple-element.142) | copy-start | bytes 1540
  251.2 4.4 %copy-start.36 = (f32[128]{0:T(128)S(1)}, f32[128]{0:T(128)}, u32[]{:S(2)}) copy-start(f32[128]{0:T(128)} %get-tuple-element.143) | copy-start | bytes 1540
  251.2 4.4 %copy-start.37 = (f32[128]{0:T(128)S(1)}, f32[128]{0:T(128)}, u32[]{:S(2)}) copy-start(f32[128]{0:T(128)} %get-tuple-element.144) | copy-start | bytes 1540
  251.2 4.4 %copy-start.38 = (f32[128]{0:T(128)S(1)}, f32[128]{0:T(128)}, u32[]{:S(2)}) copy-start(f32[128]{0:T(128)} %get-tuple-element.145) | copy-start | bytes 1540
  251.2 4.4 %copy-start.39 = (f32[128]{0:T(128)S(1)}, f32[128]{0:T(128)}, u32[]{:S(2)}) copy-start(f32[128]{0:T(128)} %get-tuple-element.146) | copy-start | bytes 1540
  251.3 4.4 %copy-start.40 = (f32[128]{0:T(128)S(1)}, f32[128]{0:T(128)}, u32[]{:S(2)}) copy-start(f32[128]{0:T(128)} %get-tuple-element.147) | copy-start | bytes 1540
  251.3 4.4 %copy-start.41 = (f32[128]{0:T(128)S(1)}, f32[128]{0:T(128)}, u32[]{:S(2)}) copy-start(f32[128]{0:T(128)} %get-tuple-element.148) | copy-start | bytes 1540
  251.3 16.3 %copy-start.4 = (f32[1,128,256]{2,1,0:T(8,128)S(1)}, f32[1,128,256]{2,1,0:T(8,128)}, u32[]{:S(2)}) copy-start(f32[1,128,256]{2,1,0:T(8,128)} %fusion.53) | copy-start | bytes 393220
  252.5 40.9 %copy-start.9 = (f32[16,1,64,256]{3,2,1,0:T(8,128)S(1)}, f32[16,1,64,256]{3,2,1,0:T(8,128)}, u32[]{:S(2)}) copy-start(f32[16,1,64,256]{3,2,1,0:T(8,128)} %get-tuple-element.53) | copy-start | bytes 3145732
  252.5 42.1 %copy-start.8 = (bf16[2048,128]{1,0:T(8,128)(2,1)S(1)}, bf16[2048,128]{1,0:T(8,128)(2,1)}, u32[]{:S(2)}) copy-start(bf16[2048,128]{1,0:T(8,128)(2,1)} %param.23) | copy-start | bytes 1572868
  252.6 42.1 %copy-start.44 = (f32[128]{0:T(128)S(1)}, f32[128]{0:T(128)}, u32[]{:S(2)}) copy-start(f32[128]{0:T(128)} %param.30) | copy-start | bytes 1540
  252.6 2.9 collective-permute-start
  259.1 13.4 %all-to-all-start = ((f32[8,1,2048]{2,1,0:T(1,128)}), f32[8,1,2048]{2,1,0:T(1,128)S(1)}, u32[]{:S(2)}, u32[]{:S(2)}) async-start(f32[8,1,2048]{2,1,0:T(1,128)} %broadcast_in_dim.36), calls=%async_computation | async-start | bytes 131072 | tf_op jit(solution)/shard_map/all_to_all | solution.py:43
  267.6 89.4 %reduce-scatter.2.cloned.1.call-start = ((), (), s32[]{:S(2)}) async-start(), calls=%async_computation.3 | async-start | bytes 4718592 | tf_op jit(solution)/shard_map/reduce_scatter | solution.py:222
  294.7 10.0 %copy-start.6 = (bf16[128,2048]{1,0:T(8,128)(2,1)S(1)}, bf16[128,2048]{1,0:T(8,128)(2,1)}, u32[]{:S(2)}) copy-start(bf16[128,2048]{1,0:T(8,128)(2,1)} %param.35) | copy-start | bytes 1572868
  294.7 10.0 %copy-start.7 = (bf16[2048,128]{1,0:T(8,128)(2,1)S(1)}, bf16[2048,128]{1,0:T(8,128)(2,1)}, u32[]{:S(2)}) copy-start(bf16[2048,128]{1,0:T(8,128)(2,1)} %param.26) | copy-start | bytes 1572868
  294.7 9.9 %copy-start.42 = (f32[128]{0:T(128)S(1)}, f32[128]{0:T(128)}, u32[]{:S(2)}) copy-start(f32[128]{0:T(128)} %param.33) | copy-start | bytes 1540
  294.7 9.9 %copy-start.43 = (f32[128]{0:T(128)S(1)}, f32[128]{0:T(128)}, u32[]{:S(2)}) copy-start(f32[128]{0:T(128)} %param.32) | copy-start | bytes 1540
Sparse Core Ops, SparseCore 0:
  9.2 42.2 all-gather.4
  247.5 36.0 all-gather.6
  315.8 41.1 reduce-scatter.1
where the time goes:
time: 368 us; the launch traced here: 364 us
  other arithmetic  108 us (29%)
  waiting for transfers between devices  98.9 us (27%)
  matrix products  84.4 us (23%)
  local copies, waits for them, and re-layouts  24.7 us (7%)
  between operations  14.6 us (4%)
  blocking collectives  11.1 us (3%)
  starting transfers between devices  10.7 us (3%)
  loops' own time  10.6 us (3%)
    another operation x4, other arithmetic, block_terms(): jax.scipy.linalg.solve_triangular(identity + lower, right, lower=True, un...  78.7 us
    reduce_scatter x1, waiting for transfers between devices, local(): lax.psum_scatter((summed + jnp.dot(conv_mixed, out_conv, preferred_elemen...  41.4 us
    all_gather x1, waiting for transfers between devices, local(): piece = lax.all_gather(tokens, 'tp', axis=1, tiled=True)  40.4 us
    dot_general x16, matrix products, advance(): output = output + jnp.einsum('hcs,hse->hce', scores_block, fresh)  23.6 us
    exp x16, other arithmetic, advance(): jnp.exp(log_block)[..., None]  20.1 us
    dot_general x7, matrix products, local(): jnp.dot(piece, weight, preferred_element_type=jnp.float32)  15.6 us
    all_gather x1, blocking collectives, prefix_by_axis(): pieces = lax.all_gather(so_far, axis)  11.1 us
    all_gather x1, waiting for transfers between devices, prefix_by_axis(): pieces = lax.all_gather(so_far, axis)  11 us
  transfers between devices with their start and end apart: 5, of which 5 were waited for; matrix products, arithmetic and copies ran while one was open for 3% of the time, Pallas kernels for 0%

commit v1 on v0

v1 whole, which is shorter than its diff:
```python
import jax
import jax.numpy as jnp
from jax import lax
from jax.experimental import pallas as pl
from jax.experimental.pallas import tpu as pltpu
from jax.sharding import PartitionSpec as P

BF = jnp.bfloat16
F32 = jnp.float32
ROWS = 1024
SHARD = 256
BLK = 128
CHUNK = 512
CHUNKS = ROWS // CHUNK
HALF = CHUNK // 2
PER = CHUNK // BLK
COLS = 9 * 128
TAPS = 31
NORM = 1e-06
VAR = 1e-05
NN = ((1,), (0,))
NT = ((1,), (1,))
TN = ((0,), (0,))


def mm(a, b, dims=NN):
    return lax.dot_general(
        a.astype(BF), b.astype(BF), (dims, ((), ())), preferred_element_type=F32
    )


def iotas(shape):
    return lax.broadcasted_iota(jnp.int32, shape, 0), lax.broadcasted_iota(jnp.int32, shape, 1)


def softplus(v):
    return jnp.maximum(v, 0.0) + jnp.log1p(jnp.exp(-jnp.abs(v)))


def sigmoid(v):
    return jax.nn.sigmoid(v)


def unit_rows(v):
    return v * lax.rsqrt(jnp.sum(v * v, axis=-1, keepdims=True) + NORM)


def block_inverse(lows):
    row, col = iotas((BLK, BLK))
    eye = (row == col).astype(F32)
    parts = [eye - jnp.where((row // 2 == col // 2), low, 0.0) for low in lows]
    m = 2
    while m < BLK:
        pick = (row // (2 * m) == col // (2 * m)) & (row // m != col // m)
        packed = [p.astype(BF) for p in parts]
        inner = [mm(jnp.where(pick, low, 0.0), p) for low, p in zip(lows, packed)]
        parts = [t - mm(p, i) for t, p, i in zip(parts, packed, inner)]
        m *= 2
    return parts


def kernel(
    x, wq, wk, wv, wdg, wgv, wgg, wcg, wb, wd, dlog, hgain, taps, lng, lns, od, oc,
    out,
    xg, w, wo, qs, ks, vs, dgs, cgs, bes, lds, pad, filt, qcs, ocs, mn, mnx, mnz, s4s, s4r,
    halo_s, halo_r, sts, str_, dms, cms, dmr, cmr,
    wsem, gs, gr, os_, or_, xs, xr, zs, zr, fs, fr, hs, hr, ss, sr, ds_, dr, cs, cr,
):
    sp = lax.axis_index("sp")
    t = lax.axis_index("tp")
    y, c = t // 2, t % 2
    z, xx = sp // 4, sp % 4
    zq, zi = z // 4, z % 4
    right = ((y + 1) % 4) * 2 + c
    left = ((y + 3) % 4) * 2 + c
    opp = ((y + 2) % 4) * 2 + c
    mate = y * 2 + (1 - c)

    def at_tp(k):
        return {"sp": sp, "tp": k}

    def at_sp(k):
        return {"sp": k, "tp": t}

    wrefs = (wq, wk, wv, wdg, wgv, wgg, wcg)
    wcopies = [
        pltpu.make_async_copy(ref, w.at[:, k * 128 : (k + 1) * 128], wsem.at[k])
        for k, ref in enumerate(wrefs)
    ]
    own_rows = pl.ds(pl.multiple_of(t * 128, 128), 128)
    wcopies.append(pltpu.make_async_copy(od, wo.at[0, own_rows, :], wsem.at[7]))
    wcopies.append(pltpu.make_async_copy(oc, wo.at[1, own_rows, :], wsem.at[8]))

    def cols_of(k):
        return pl.ds(pl.multiple_of(k * SHARD, SHARD), SHARD)

    xcopy = pltpu.make_async_copy(x, xg.at[:, cols_of(t)], wsem.at[9])
    xcopy.start()
    for cp in wcopies:
        cp.start()

    bar = pltpu.get_barrier_semaphore()
    peers = [at_tp((t + d) % 8) for d in range(1, 8)]
    peers += [at_sp(z * 4 + (xx + d) % 4) for d in range(1, 4)]
    peers += [at_sp((zq * 4 + (zi + d) % 4) * 4 + xx) for d in range(1, 4)]
    peers += [at_sp(((z + 4) % 8) * 4 + xx), at_sp((sp + 1) % 32), at_sp((sp + 31) % 32)]
    for peer in peers:
        pl.semaphore_signal(bar, inc=1, device_id=peer, device_id_type=pl.DeviceIdType.MESH)
    pl.semaphore_wait(bar, len(peers))

    def send(src, dst, ssem, rsem, to):
        return pltpu.make_async_remote_copy(
            src_ref=src, dst_ref=dst, send_sem=ssem, recv_sem=rsem,
            device_id=to, device_id_type=pl.DeviceIdType.MESH,
        )

    def gat(kind, r):
        base = r * CHUNK
        whole = pl.ds(pl.multiple_of(base, CHUNK), CHUNK)
        first = pl.ds(pl.multiple_of(base, HALF), HALF)
        second = pl.ds(pl.multiple_of(base + HALF, HALF), HALF)
        rows = (whole, whole, whole, first, second, whole, whole, first, second)[kind]
        shard = (t, t, t, left, right, left, right, opp, opp)[kind]
        to = (right, left, mate, right, left, mate, mate, mate, mate)[kind]
        dst = xg.at[rows, cols_of(shard)]
        src = x.at[rows, :] if kind < 3 else dst
        return send(src, dst, gs.at[kind, r], gr.at[kind, r], at_tp(to))

    def own(r):
        for kind in (0, 1, 2):
            gat(kind, r).start()

    def relay1(r):
        gat(0, r).wait_recv()
        gat(3, r).start()
        gat(5, r).start()
        gat(1, r).wait_recv()
        gat(4, r).start()
        gat(6, r).start()

    def relay2(r):
        gat(3, r).wait_recv()
        gat(7, r).start()
        gat(4, r).wait_recv()
        gat(8, r).start()

    def owg(kind):
        shard = (t, t, t, left, right, left, right, opp, opp)[kind]
        to = (right, left, mate, right, left, mate, mate, mate, mate)[kind]
        rows = pl.ds(pl.multiple_of(shard * 128, 128), 128)
        if kind in (3, 7):
            ref = wo.at[1, rows, :]
        elif kind in (4, 8):
            ref = wo.at[0, rows, :]
        else:
            ref = wo.at[:, rows, :]
        return send(ref, ref, os_.at[kind], or_.at[kind], at_tp(to))

    own(0)
    own(1)

    pick = (lax.broadcasted_iota(jnp.int32, (8, 128), 0) == t).astype(BF)
    w[:, 896:1024] = mm(wb[...], pick).astype(BF)
    w[:, 1024:1152] = mm(wd[...], pick).astype(BF)
    rate = jnp.exp(jnp.full((1, 128), dlog[t], F32))
    row, col = iotas((BLK, BLK))
    causal = row >= col
    strict = row > col
    tri = causal.astype(F32)
    mn[:, :128] = (row == col).astype(F32)
    mn[:, 128:] = jnp.zeros((BLK, BLK), F32)

    for cp in wcopies[:7]:
        cp.wait()
    xcopy.wait()

    def project(r):
        for sub in range(CHUNK // 256):
            rows = pl.ds(pl.multiple_of(r * CHUNK + sub * 256, 256), 256)
            xr_ = xg[rows, :]
            xf = xr_.astype(F32)
            inv = lax.rsqrt(jnp.sum(xf * xf, axis=1, keepdims=True) / 2048.0 + NORM)
            raw = []
            for n in range(0, COLS, 256):
                width = min(256, COLS - n)
                d = jnp.dot(xr_, w[:, n : n + width], preferred_element_type=F32) * inv
                for k in range(width // 128):
                    raw.append(d[:, k * 128 : (k + 1) * 128])
            q, k, v, dg, gv, gg, cg = [a.astype(BF).astype(F32) for a in raw[:7]]
            qs[rows, :] = unit_rows(q) * (128.0 ** -0.5)
            ks[rows, :] = unit_rows(k)
            vs[rows, :] = v
            dgs[rows, :] = dg * sigmoid(dg)
            cgs[rows, :] = cg * sigmoid(cg)
            bes[rows, :] = sigmoid(raw[7])
            lds[rows, :] = -rate * softplus(raw[8])
            below = pl.ds(pl.multiple_of(r * CHUNK + sub * 256 + 32, 32), 256)
            pad[below, :] = (gv * sigmoid(gg)).astype(BF).astype(F32)

    def delta(r):
        spans = [pl.ds(pl.multiple_of(r * CHUNK + b * BLK, BLK), BLK) for b in range(PER)]
        sums, lows, scores = [], [], []
        for rows in spans:
            total = lax.dot_general(
                tri, lds[rows, :], (NN, ((), ())),
                precision=lax.Precision.HIGHEST, preferred_element_type=F32,
            )
            spread = total - total.T
            damp = jnp.where(causal, jnp.exp(jnp.where(causal, spread, 0.0)), 0.0)
            kb = ks[rows, :].astype(BF)
            both = mm(jnp.concatenate([kb, qs[rows, :].astype(BF)], axis=0), kb, NT)
            lows.append(jnp.where(strict, both[:BLK] * bes[rows, :] * damp, 0.0))
            scores.append(both[BLK:] * damp)
            sums.append(total)
        inverses = block_inverse(lows)
        later = []
        for rows, total, score, inv in zip(spans, sums, scores, inverses):
            grow = jnp.exp(total)
            kv, be = ks[rows, :], bes[rows, :]
            rhs = jnp.concatenate([vs[rows, :] * be, kv * be * grow], axis=1)
            solved = mm(inv, rhs).astype(BF)
            mixed = mm(score, solved)
            tail = total[BLK - 1 : BLK, :]
            fresh = mm(kv * jnp.exp(tail - total), solved, TN)
            later.append(
                (
                    jnp.concatenate([qs[rows, :] * grow - mixed[:, 128:], fresh[:, 128:]], axis=0),
                    mixed[:, :128], fresh[:, :128], jnp.exp(tail),
                )
            )
        state = mn[...]
        for rows, (lhs, o_here, n_here, fade) in zip(spans, later):
            moved = mm(lhs, state)
            qcs[rows, :] = moved[:BLK, :128]
            ocs[rows, :] = moved[:BLK, 128:] + o_here
            m_next = state[:, :128] * fade - moved[BLK:, :128]
            n_next = state[:, 128:] * fade - moved[BLK:, 128:] + n_here
            state = jnp.concatenate([m_next, n_next], axis=1)
        mn[...] = state

    def compute(r):
        for kind in (2, 5, 6, 7, 8):
            gat(kind, r).wait_recv()
        project(r)
        delta(r)

    relay1(0)
    relay1(1)
    relay2(0)
    for kk in (7, 8):
        wcopies[kk].wait()

    @pl.loop(0, CHUNKS)
    def _(r):
        compute(r)

        @pl.when(r == 0)
        def _():
            relay2(1)

    own_x = mn[...].astype(BF)
    mnx[xx] = own_x

    def xsend(d):
        return send(mnx.at[xx], mnx.at[xx], xs.at[d - 1], xr.at[d - 1],
                    at_sp(z * 4 + (xx + d) % 4))

    for d in (1, 2, 3):
        xsend(d).start()
    halo_s[...] = pad[ROWS : ROWS + 32, :].astype(BF)
    hcopy = send(halo_s, halo_r, hs, hr, at_sp((sp + 1) % 32))
    hcopy.start()
    for kind in (0, 1, 2):
        owg(kind).start()

    tapf = taps[...].astype(F32)

    def conv_rows(i):
        acc = jnp.zeros((64, 128), F32)
        for j in range(TAPS):
            acc = acc + pad[pl.ds(i * 64 + 2 + j, 64), :] * tapf[j : j + 1, :]
        filt[pl.ds(pl.multiple_of(i * 64, 64), 64), :] = acc

    @pl.loop(1, ROWS // 64)
    def _(i):
        conv_rows(i)

    hcopy.wait_recv()
    keep = (sp > 0).astype(F32)
    pad[0:32, :] = halo_r[...].astype(F32) * keep
    conv_rows(0)
    for b in range(ROWS // BLK):
        lanes = slice(b * BLK, (b + 1) * BLK)
        ft = filt[lanes, :].T
        sts[0:1, lanes] = jnp.sum(ft, axis=0, keepdims=True)
        sts[1:2, lanes] = jnp.sum(ft * ft, axis=0, keepdims=True)

    def ssend(d):
        return send(sts, str_.at[t], ss.at[d - 1], sr.at[d - 1], at_tp((t + d) % 8))

    for d in range(1, 8):
        ssend(d).start()
    str_[t] = sts[...]

    def chain(slots, mine):
        total = slots[0].astype(F32)
        m_in = jnp.where(mine > 0, total[:, :128], (row == col).astype(F32))
        n_in = jnp.where(mine > 0, total[:, 128:], 0.0)
        for k in (1, 2, 3):
            piece = slots[k]
            moved = mm(piece[:, :128], total)
            total = jnp.concatenate(
                [moved[:, :128], moved[:, 128:] + piece[:, 128:].astype(F32)], axis=1
            )
            if k < 3:
                m_in = jnp.where(mine > k, total[:, :128], m_in)
                n_in = jnp.where(mine > k, total[:, 128:], n_in)
        return m_in, n_in, total

    for d in (1, 2, 3):
        xsend(d).wait_recv()
    mxp, nxp, xtotal = chain(mnx, xx)
    mnz[zi] = xtotal.astype(BF)

    def zsend(d):
        return send(mnz.at[zi], mnz.at[zi], zs.at[d - 1], zr.at[d - 1],
                    at_sp((zq * 4 + (zi + d) % 4) * 4 + xx))

    for d in (1, 2, 3):
        zsend(d).start()

    owg(0).wait_recv()
    owg(3).start()
    owg(5).start()
    owg(1).wait_recv()
    owg(4).start()
    owg(6).start()

    for d in range(1, 8):
        ssend(d).wait_recv()
    both = str_[0]
    for k in range(1, 8):
        both = both + str_[k]
    center = both[0:1, :] / 1024.0
    variance = jnp.maximum(both[1:2, :] / 1024.0 - center * center, 0.0)
    scale = lax.rsqrt(variance + VAR)
    for b in range(ROWS // BLK):
        lanes = slice(b * BLK, (b + 1) * BLK)
        cen = jnp.broadcast_to(center[:, lanes], (BLK, BLK)).T
        sca = jnp.broadcast_to(scale[:, lanes], (BLK, BLK)).T
        normed = (filt[lanes, :] - cen) * sca * lng[...] + lns[...]
        cms[lanes, :] = (normed * sigmoid(normed) * cgs[lanes, :]).astype(BF)

    def a2a(src, dst, s_sem, r_sem, d):
        to = (t + d) % 8
        rows = pl.ds(pl.multiple_of(to * BLK, BLK), BLK)
        return send(src.at[rows, :], dst.at[t], s_sem.at[d - 1], r_sem.at[d - 1], at_tp(to))

    for d in range(1, 8):
        a2a(cms, cmr, cs, cr, d).start()
    cmr[t] = cms[own_rows, :]

    for d in (1, 2, 3):
        zsend(d).wait_recv()
    mzp, nzp, ztotal = chain(mnz, zi)
    s4s[...] = ztotal[:, 128:].astype(BF)
    fcopy = send(s4s, s4r, fs, fr, at_sp(((z + 4) % 8) * 4 + xx))
    fcopy.start()
    moved = mm(mxp, jnp.concatenate([mzp, nzp], axis=1))
    mpre, npre = moved[:, :128], moved[:, 128:] + nxp
    fcopy.wait_recv()
    begin = s4r[...].astype(F32) * (zq > 0).astype(F32)
    carried = mm(mpre, begin) + npre

    for b in range(ROWS // BLK):
        lanes = slice(b * BLK, (b + 1) * BLK)
        o = ocs[lanes, :] + mm(qcs[lanes, :], carried)
        o = o * lax.rsqrt(jnp.mean(o * o, axis=-1, keepdims=True) + NORM) * hgain[...]
        dms[lanes, :] = (o * dgs[lanes, :]).astype(BF)
    for d in range(1, 8):
        a2a(dms, dmr, ds_, dr, d).start()
    dmr[t] = dms[own_rows, :]

    owg(3).wait_recv()
    owg(7).start()
    owg(4).wait_recv()
    owg(8).start()
    for d in range(1, 8):
        a2a(cms, cmr, cs, cr, d).wait_recv()
    for kind in (2, 5, 6, 7, 8):
        owg(kind).wait_recv()
    for d in range(1, 8):
        a2a(dms, dmr, ds_, dr, d).wait_recv()

    lhs_d = jnp.concatenate([dmr[k] for k in range(8)], axis=1)
    lhs_c = jnp.concatenate([cmr[k] for k in range(8)], axis=1)

    @pl.loop(0, 8)
    def _(n):
        lanes = pl.ds(pl.multiple_of(n * 256, 256), 256)
        acc = jnp.dot(lhs_d, wo[0, :, lanes], preferred_element_type=F32)
        acc = acc + jnp.dot(lhs_c, wo[1, :, lanes], preferred_element_type=F32)
        out[:, lanes] = acc.astype(BF)

    for r in range(CHUNKS):
        for kind in range(9):
            gat(kind, r).wait_send()
    for kind in range(9):
        owg(kind).wait_send()
    for d in (1, 2, 3):
        xsend(d).wait_send()
        zsend(d).wait_send()
    hcopy.wait_send()
    fcopy.wait_send()
    for d in range(1, 8):
        ssend(d).wait_send()
        a2a(cms, cmr, cs, cr, d).wait_send()
        a2a(dms, dmr, ds_, dr, d).wait_send()


def local(*args):
    (tokens, w_query, w_key, w_value, w_delta_gate, w_glu_value, w_glu_gate, w_conv_gate,
     w_beta, w_decay, decay_log, head_gain, conv_taps, ln_gain, ln_shift, out_delta,
     out_conv) = args
    vm = pl.BlockSpec(memory_space=pltpu.VMEM)
    hb = pl.BlockSpec(memory_space=pl.ANY)
    sm = pl.BlockSpec(memory_space=pltpu.SMEM)
    big = lambda kind: pltpu.VMEM((ROWS, 128), kind)
    dma = pltpu.SemaphoreType.DMA
    return pl.pallas_call(
        kernel,
        out_shape=jax.ShapeDtypeStruct((BLK, 2048), BF),
        in_specs=[vm] + [hb] * 7 + [vm, vm, sm] + [vm] * 4 + [hb, hb],
        out_specs=vm,
        scratch_shapes=[
            pltpu.VMEM((ROWS, 2048), BF),
            pltpu.VMEM((2048, COLS), BF),
            pltpu.VMEM((2, 1024, 2048), BF),
            big(F32), big(F32), big(F32), big(F32), big(F32), big(F32), big(F32),
            pltpu.VMEM((ROWS + 32, 128), F32),
            big(F32), big(F32), big(F32),
            pltpu.VMEM((BLK, 256), F32),
            pltpu.VMEM((4, BLK, 256), BF),
            pltpu.VMEM((4, BLK, 256), BF),
            pltpu.VMEM((BLK, BLK), BF),
            pltpu.VMEM((BLK, BLK), BF),
            pltpu.VMEM((32, 128), BF),
            pltpu.VMEM((32, 128), BF),
            pltpu.VMEM((2, ROWS), F32),
            pltpu.VMEM((8, 2, ROWS), F32),
            big(BF), big(BF),
            pltpu.VMEM((8, BLK, BLK), BF),
            pltpu.VMEM((8, BLK, BLK), BF),
            dma((10,)),
            dma((9, CHUNKS)), dma((9, CHUNKS)),
            dma((9,)), dma((9,)),
            dma((3,)), dma((3,)), dma((3,)), dma((3,)),
            dma, dma, dma, dma,
            dma((7,)), dma((7,)), dma((7,)), dma((7,)), dma((7,)), dma((7,)),
        ],
        compiler_params=pltpu.CompilerParams(
            collective_id=0, has_side_effects=True, vmem_limit_bytes=60 * 1024 * 1024
        ),
        name="layer",
    )(
        tokens, w_query, w_key, w_value, w_delta_gate, w_glu_value, w_glu_gate, w_conv_gate,
        w_beta, w_decay, decay_log, head_gain.reshape(1, 128), conv_taps,
        ln_gain.reshape(1, 128), ln_shift.reshape(1, 128), out_delta, out_conv,
    )


def solution(mesh):
    cut = P(None, "tp")
    placed = (P("sp", "tp"),) + (cut,) * 7 + (P(),) * 4 + (
        cut, P("tp"), P("tp"), P("tp", None), P("tp", None),
    )
    return jax.shard_map(
        local, mesh=mesh, in_specs=placed, out_specs=P(("sp", "tp"), None), check_vma=False
    )
```

time: 368 us -> 95.2 us (0.26); the launches traced: 364 us -> 95 us
  other arithmetic: 108 us -> 0 us
  waiting for transfers between devices: 98.9 us -> 0 us
  Pallas kernels: 0 us -> 90.4 us
  matrix products: 84.4 us -> 0 us
  local copies, waits for them, and re-layouts: 24.7 us -> 4.65 us
  between operations: 14.6 us -> 0.01 us
  blocking collectives: 11.1 us -> 0 us
  starting transfers between devices: 10.7 us -> 0 us
  loops' own time: 10.6 us -> 0 us
    pallas_call x0 -> x1, Pallas kernels: none -> 90.4 us  [local(): pl.pallas_call(kernel, out_shape=jax.ShapeDtypeStruct((BLK, 2048), BF), i...]
    dot_general x89 -> x0, matrix products: 83.4 us -> none  [the longest x16 23.6 us: advance(): output = output + jnp.einsum('hcs,hse->hce', scores_block, fresh)]
    another operation x5 -> x0, other arithmetic: 79 us -> none  [the longest x4 78.7 us: block_terms(): jax.scipy.linalg.solve_triangular(identity + lower, right, lower=True, un...]
    all_gather x2 -> x0, waiting for transfers between devices: 51.4 us -> none  [the longest x1 40.4 us: local(): piece = lax.all_gather(tokens, 'tp', axis=1, tiled=True)]
    reduce_scatter x1 -> x0, waiting for transfers between devices: 41.4 us -> none  [local(): lax.psum_scatter((summed + jnp.dot(conv_mixed, out_conv, preferred_elemen...]
    exp x16 -> x0, other arithmetic: 20.1 us -> none  [advance(): jnp.exp(log_block)[..., None]]
    all_gather x1 -> x0, blocking collectives: 11.1 us -> none  [prefix_by_axis(): pieces = lax.all_gather(so_far, axis)]
    slice x20 -> x0, local copies, waits for them, and re-layouts: 11 us -> none  [the longest x16 9.86 us: advance(): tail_log = log_block[:, -1:]]
  transfers between devices with their start and end apart: 5 -> 0, of which waited for: 5 -> 0; matrix products, arithmetic and copies ran while one was open for 3% -> 0% of each run, Pallas kernels for 0% -> 0%
where the time goes in v1:
time: 95.2 us; the launch traced here: 95 us
  Pallas kernels  90.4 us (95%)
  local copies, waits for them, and re-layouts  4.65 us (5%)
    pallas_call x1, Pallas kernels, local(): pl.pallas_call(kernel, out_shape=jax.ShapeDtypeStruct((BLK, 2048), BF), i...  90.4 us
    unnamed x5, local copies, waits for them, and re-layouts  4.65 us

profile of v1, /device:TPU:1, one launch (start us, length us, event | category | flops | bytes accessed | tf_op | source)
XLA Modules:
  0.0 95.0 jit_solution(12294507334380641484)
XLA Ops:
  0.0 0.0 copy-start
  0.0 1.8 %copy.18.wb = bf16[2048,8]{1,0:T(8,128)(2,1)} copy(bf16[2048,8]{0,1:T(8,128)(2,1)} %param.25) | data formatting | bytes 65536 | tf_op args[8]
  1.8 0.0 copy-done
  1.8 1.0 %copy.19.wd = bf16[2048,8]{1,0:T(8,128)(2,1)} copy(bf16[2048,8]{0,1:T(8,128)(2,1)S(1)} %copy-done) | data formatting | bytes 65536 | tf_op args[9]
  2.8 90.4 %layer.1 = bf16[128,2048]{1,0:T(8,128)(2,1)} custom-call(bf16[1024,256]{1,0:T(8,128)(2,1)} %x.1, bf16[2048,128]{1,0:T(8,128)(2,1)} %wq.1, bf16[2048,128]{1,0:T(8,128)(2,1)} %wk.1, bf16[2048,128]{1,0:T(8,128)(2,1)} %wv.1, bf16[2048,128]{1,0:T(8,128)(2,1)} %wdg.1, bf16[2048,128]{1,0:T(8,128)(2,1)} %wgv.1, bf16[2048,128]{1,0:T(8,128)(2,1)} %wgg.1, ...), custom_call_target="tpu_custom_call" | custom-call | tf_op jit(solution)/shard_map/layer/pallas_call | solution.py:430
  93.2 1.9 %copy.21 = bf16[128,2048]{1,0:T(8,128)(2,1)} copy(bf16[128,2048]{1,0:T(8,128)(2,1)} %layer.1) | data formatting | bytes 1048576
Async XLA Ops:
  0.0 1.8 %copy-start = (bf16[2048,8]{0,1:T(8,128)(2,1)S(1)}, bf16[2048,8]{0,1:T(8,128)(2,1)}, u32[]{:S(2)}) copy-start(bf16[2048,8]{0,1:T(8,128)(2,1)} %param.26) | copy-start | bytes 98308

commit v2 on v1

--- a/solution.py
+++ b/solution.py
@@ -10,11 +10,13 @@
 ROWS = 1024
 SHARD = 256
 BLK = 128
-CHUNK = 512
+CHUNK = 256
 CHUNKS = ROWS // CHUNK
 HALF = CHUNK // 2
-PER = CHUNK // BLK
-COLS = 9 * 128
+GROUP = 512
+PER = GROUP // BLK
+COLS = 8 * 128
+MOVES = 31
 TAPS = 31
 NORM = 1e-06
 VAR = 1e-05
@@ -63,8 +65,8 @@
     x, wq, wk, wv, wdg, wgv, wgg, wcg, wb, wd, dlog, hgain, taps, lng, lns, od, oc,
     out,
     xg, w, wo, qs, ks, vs, dgs, cgs, bes, lds, pad, filt, qcs, ocs, mn, mnx, mnz, s4s, s4r,
-    halo_s, halo_r, sts, str_, dms, cms, dmr, cmr,
-    wsem, gs, gr, os_, or_, xs, xr, zs, zr, fs, fr, hs, hr, ss, sr, ds_, dr, cs, cr,
+    halo_s, halo_r, sts, str_, dms, cms, dmr, cmr, stage,
+    wsem, gs, gr, os_, or_, xs, xr, zs, zr, fs, fr, hs, hr, ss, sr, ds_, dr, cs, cr, osem,
 ):
     sp = lax.axis_index("sp")
     t = lax.axis_index("tp")
@@ -123,8 +125,7 @@
         shard = (t, t, t, left, right, left, right, opp, opp)[kind]
         to = (right, left, mate, right, left, mate, mate, mate, mate)[kind]
         dst = xg.at[rows, cols_of(shard)]
-        src = x.at[rows, :] if kind < 3 else dst
-        return send(src, dst, gs.at[kind, r], gr.at[kind, r], at_tp(to))
+        return send(dst, dst, gs.at[kind, r], gr.at[kind, r], at_tp(to))
 
     def own(r):
         for kind in (0, 1, 2):
@@ -144,24 +145,52 @@
         gat(4, r).wait_recv()
         gat(8, r).start()
 
-    def owg(kind):
-        shard = (t, t, t, left, right, left, right, opp, opp)[kind]
-        to = (right, left, mate, right, left, mate, mate, mate, mate)[kind]
-        rows = pl.ds(pl.multiple_of(shard * 128, 128), 128)
-        if kind in (3, 7):
-            ref = wo.at[1, rows, :]
-        elif kind in (4, 8):
-            ref = wo.at[0, rows, :]
-        else:
-            ref = wo.at[:, rows, :]
-        return send(ref, ref, os_.at[kind], or_.at[kind], at_tp(to))
-
+    def rows_of(shard, off, n):
+        return pl.ds(pl.multiple_of(shard * 128 + off, 16), n)
+
+    near = (left, right, opp)
+    xr_id = at_sp(z * 4 + (xx + 1) % 4)
+    xl_id = at_sp(z * 4 + (xx + 3) % 4)
+    x_left, x_right, x_opp = (xx + 3) % 4, (xx + 1) % 4, (xx + 2) % 4
+    moves = {"m": (wo.at[:, rows_of(t, 0, 128), :], at_tp(mate))}
+    for h in (0, 1):
+        a_own = wo.at[0, rows_of(t, 64 * h, 64), :]
+        moves["ar", h] = (a_own, at_tp(right))
+        moves["al", h] = (a_own, at_tp(left))
+        moves["afr", h] = (wo.at[0, rows_of(left, 64 * h, 32), :], at_tp(right))
+        moves["afl", h] = (wo.at[0, rows_of(right, 64 * h + 32, 32), :], at_tp(left))
+    for j in range(3):
+        moves["am", j] = (wo.at[0, rows_of(near[j], 0, 128), :], at_tp(mate))
+    b_own = wo.at[1, rows_of(t, 32 * xx, 32), :]
+    moves["br"] = (b_own, at_tp(right))
+    moves["bl"] = (b_own, at_tp(left))
+    moves["bfr"] = (wo.at[1, rows_of(left, 32 * xx, 16), :], at_tp(right))
+    moves["bfl"] = (wo.at[1, rows_of(right, 32 * xx + 16, 16), :], at_tp(left))
+    for j in range(3):
+        b_mine = wo.at[1, rows_of(near[j], 32 * xx, 32), :]
+        moves["xr", j] = (b_mine, xr_id)
+        moves["xl", j] = (b_mine, xl_id)
+        moves["xfr", j] = (wo.at[1, rows_of(near[j], 32 * x_left, 16), :], xr_id)
+        moves["xfl", j] = (wo.at[1, rows_of(near[j], 32 * x_right + 16, 16), :], xl_id)
+        moves["xm", j] = (wo.at[1, rows_of(near[j], 0, 128), :], at_tp(mate))
+    assert len(moves) == MOVES
+
+    def move(*key):
+        key = key if len(key) > 1 else key[0]
+        ref, to = moves[key]
+        k = list(moves).index(key)
+        return send(ref, ref, os_.at[k], or_.at[k], to)
+
+    xcopy.wait()
     own(0)
     own(1)
 
     pick = (lax.broadcasted_iota(jnp.int32, (8, 128), 0) == t).astype(BF)
-    w[:, 896:1024] = mm(wb[...], pick).astype(BF)
-    w[:, 1024:1152] = mm(wd[...], pick).astype(BF)
+    lane = lax.broadcasted_iota(jnp.int32, (8, 128), 1)
+    w[:, 896:1024] = (
+        mm(wb[...], jnp.where(lane < 64, pick, 0), TN)
+        + mm(wd[...], jnp.where(lane < 64, 0, pick), TN)
+    ).astype(BF)
     rate = jnp.exp(jnp.full((1, 128), dlog[t], F32))
     row, col = iotas((BLK, BLK))
     causal = row >= col
@@ -172,33 +201,31 @@
 
     for cp in wcopies[:7]:
         cp.wait()
-    xcopy.wait()
 
     def project(r):
-        for sub in range(CHUNK // 256):
-            rows = pl.ds(pl.multiple_of(r * CHUNK + sub * 256, 256), 256)
-            xr_ = xg[rows, :]
-            xf = xr_.astype(F32)
-            inv = lax.rsqrt(jnp.sum(xf * xf, axis=1, keepdims=True) / 2048.0 + NORM)
-            raw = []
-            for n in range(0, COLS, 256):
-                width = min(256, COLS - n)
-                d = jnp.dot(xr_, w[:, n : n + width], preferred_element_type=F32) * inv
-                for k in range(width // 128):
-                    raw.append(d[:, k * 128 : (k + 1) * 128])
-            q, k, v, dg, gv, gg, cg = [a.astype(BF).astype(F32) for a in raw[:7]]
-            qs[rows, :] = unit_rows(q) * (128.0 ** -0.5)
-            ks[rows, :] = unit_rows(k)
-            vs[rows, :] = v
-            dgs[rows, :] = dg * sigmoid(dg)
-            cgs[rows, :] = cg * sigmoid(cg)
-            bes[rows, :] = sigmoid(raw[7])
-            lds[rows, :] = -rate * softplus(raw[8])
-            below = pl.ds(pl.multiple_of(r * CHUNK + sub * 256 + 32, 32), 256)
-            pad[below, :] = (gv * sigmoid(gg)).astype(BF).astype(F32)
+        rows = pl.ds(pl.multiple_of(r * CHUNK, CHUNK), CHUNK)
+        xr_ = xg[rows, :]
+        xf = xr_.astype(F32)
+        inv = lax.rsqrt(jnp.sum(xf * xf, axis=1, keepdims=True) / 2048.0 + NORM)
+        raw = []
+        for n in range(0, COLS, 256):
+            d = jnp.dot(xr_, w[:, n : n + 256], preferred_element_type=F32) * inv
+            raw += [d[:, :128], d[:, 128:]]
+        q, k, v, dg, gv, gg, cg = [a.astype(BF).astype(F32) for a in raw[:7]]
+        qs[rows, :] = unit_rows(q) * (128.0 ** -0.5)
+        ks[rows, :] = unit_rows(k)
+        vs[rows, :] = v
+        dgs[rows, :] = dg * sigmoid(dg)
+        cgs[rows, :] = cg * sigmoid(cg)
+        turned = pltpu.roll(raw[7], 64, 1)
+        low_lanes = lax.broadcasted_iota(jnp.int32, (CHUNK, 128), 1) < 64
+        bes[rows, :] = sigmoid(jnp.where(low_lanes, raw[7], turned))
+        lds[rows, :] = -rate * softplus(jnp.where(low_lanes, turned, raw[7]))
+        below = pl.ds(pl.multiple_of(r * CHUNK + 32, 32), CHUNK)
+        pad[below, :] = (gv * sigmoid(gg)).astype(BF).astype(F32)
 
     def delta(r):
-        spans = [pl.ds(pl.multiple_of(r * CHUNK + b * BLK, BLK), BLK) for b in range(PER)]
+        spans = [pl.ds(pl.multiple_of(r * GROUP + b * BLK, BLK), BLK) for b in range(PER)]
         sums, lows, scores = [], [], []
         for rows in spans:
             total = lax.dot_general(
@@ -238,25 +265,45 @@
             state = jnp.concatenate([m_next, n_next], axis=1)
         mn[...] = state
 
-    def compute(r):
+    def arrive(r):
         for kind in (2, 5, 6, 7, 8):
             gat(kind, r).wait_recv()
-        project(r)
-        delta(r)
 
     relay1(0)
+    own(2)
     relay1(1)
+    own(3)
     relay2(0)
     for kk in (7, 8):
         wcopies[kk].wait()
 
-    @pl.loop(0, CHUNKS)
-    def _(r):
-        compute(r)
-
-        @pl.when(r == 0)
+    @pl.loop(0, 2)
+    def _(p):
+        arrive(2 * p)
+        project(2 * p)
+
+        @pl.when(p == 0)
         def _():
+            relay1(2)
             relay2(1)
+
+        arrive(2 * p + 1)
+        project(2 * p + 1)
+
+        @pl.when(p == 0)
+        def _():
+            relay1(3)
+
+        delta(p)
+
+        @pl.when(p == 0)
+        def _():
+            relay2(2)
+            relay2(3)
+            for key in ("br", "bl", "m"):
+                move(key).start()
+            move("ar", 0).start()
+            move("al", 0).start()
 
     own_x = mn[...].astype(BF)
     mnx[xx] = own_x
@@ -270,8 +317,15 @@
     halo_s[...] = pad[ROWS : ROWS + 32, :].astype(BF)
     hcopy = send(halo_s, halo_r, hs, hr, at_sp((sp + 1) % 32))
     hcopy.start()
-    for kind in (0, 1, 2):
-        owg(kind).start()
+    move("br").wait_recv()
+    move("bfr").start()
+    move("bl").wait_recv()
+    move("bfl").start()
+    move("ar", 1).start()
+    move("al", 1).start()
+    for j in (0, 1):
+        move("xr", j).start()
+        move("xl", j).start()
 
     tapf = taps[...].astype(F32)
 
@@ -329,12 +383,14 @@
     for d in (1, 2, 3):
         zsend(d).start()
 
-    owg(0).wait_recv()
-    owg(3).start()
-    owg(5).start()
-    owg(1).wait_recv()
-    owg(4).start()
-    owg(6).start()
+    move("bfr").wait_recv()
+    move("bfl").wait_recv()
+    move("xr", 2).start()
+    move("xl", 2).start()
+    move("ar", 0).wait_recv()
+    move("afr", 0).start()
+    move("al", 0).wait_recv()
+    move("afl", 0).start()
 
     for d in range(1, 8):
         ssend(d).wait_recv()
@@ -368,6 +424,17 @@
     fcopy.start()
     moved = mm(mxp, jnp.concatenate([mzp, nzp], axis=1))
     mpre, npre = moved[:, :128], moved[:, 128:] + nxp
+    for j in (0, 1, 2):
+        move("xr", j).wait_recv()
+        move("xfr", j).start()
+        move("xl", j).wait_recv()
+        move("xfl", j).start()
+    move("ar", 1).wait_recv()
+    move("afr", 1).start()
+    move("am", 0).start()
+    move("al", 1).wait_recv()
+    move("afl", 1).start()
+    move("am", 1).start()
     fcopy.wait_recv()
     begin = s4r[...].astype(F32) * (zq > 0).astype(F32)
     carried = mm(mpre, begin) + npre
@@ -381,32 +448,45 @@
         a2a(dms, dmr, ds_, dr, d).start()
     dmr[t] = dms[own_rows, :]
 
-    owg(3).wait_recv()
-    owg(7).start()
-    owg(4).wait_recv()
-    owg(8).start()
+    for j in (0, 1, 2):
+        move("xfr", j).wait_recv()
+        move("xfl", j).wait_recv()
+        move("xm", j).start()
+    for h in (0, 1):
+        move("afr", h).wait_recv()
+        move("afl", h).wait_recv()
+    move("am", 2).start()
     for d in range(1, 8):
         a2a(cms, cmr, cs, cr, d).wait_recv()
-    for kind in (2, 5, 6, 7, 8):
-        owg(kind).wait_recv()
+    move("m").wait_recv()
+    for j in (0, 1, 2):
+        move("xm", j).wait_recv()
+        move("am", j).wait_recv()
     for d in range(1, 8):
         a2a(dms, dmr, ds_, dr, d).wait_recv()
 
     lhs_d = jnp.concatenate([dmr[k] for k in range(8)], axis=1)
     lhs_c = jnp.concatenate([cmr[k] for k in range(8)], axis=1)
+
+    def ocopy(n):
+        lanes = pl.ds(pl.multiple_of(n * 256, 256), 256)
+        return pltpu.make_async_copy(stage.at[n], out.at[:, lanes], osem.at[n])
 
     @pl.loop(0, 8)
     def _(n):
         lanes = pl.ds(pl.multiple_of(n * 256, 256), 256)
         acc = jnp.dot(lhs_d, wo[0, :, lanes], preferred_element_type=F32)
         acc = acc + jnp.dot(lhs_c, wo[1, :, lanes], preferred_element_type=F32)
-        out[:, lanes] = acc.astype(BF)
-
+        stage[n] = acc.astype(BF)
+        ocopy(n).start()
+
+    for n in range(8):
+        ocopy(n).wait()
     for r in range(CHUNKS):
         for kind in range(9):
             gat(kind, r).wait_send()
-    for kind in range(9):
-        owg(kind).wait_send()
+    for key in moves:
+        move(*(key if isinstance(key, tuple) else (key,))).wait_send()
     for d in (1, 2, 3):
         xsend(d).wait_send()
         zsend(d).wait_send()
@@ -430,8 +510,8 @@
     return pl.pallas_call(
         kernel,
         out_shape=jax.ShapeDtypeStruct((BLK, 2048), BF),
-        in_specs=[vm] + [hb] * 7 + [vm, vm, sm] + [vm] * 4 + [hb, hb],
-        out_specs=vm,
+        in_specs=[hb] * 8 + [vm, vm, sm] + [vm] * 4 + [hb, hb],
+        out_specs=hb,
         scratch_shapes=[
             pltpu.VMEM((ROWS, 2048), BF),
             pltpu.VMEM((2048, COLS), BF),
@@ -451,12 +531,13 @@
             big(BF), big(BF),
             pltpu.VMEM((8, BLK, BLK), BF),
             pltpu.VMEM((8, BLK, BLK), BF),
+            pltpu.VMEM((8, BLK, 256), BF),
             dma((10,)),
             dma((9, CHUNKS)), dma((9, CHUNKS)),
-            dma((9,)), dma((9,)),
+            dma((MOVES,)), dma((MOVES,)),
             dma((3,)), dma((3,)), dma((3,)), dma((3,)),
             dma, dma, dma, dma,
-            dma((7,)), dma((7,)), dma((7,)), dma((7,)), dma((7,)), dma((7,)),
+            dma((7,)), dma((7,)), dma((7,)), dma((7,)), dma((7,)), dma((7,)), dma((8,)),
         ],
         compiler_params=pltpu.CompilerParams(
             collective_id=0, has_side_effects=True, vmem_limit_bytes=60 * 1024 * 1024
@@ -464,7 +545,7 @@
         name="layer",
     )(
         tokens, w_query, w_key, w_value, w_delta_gate, w_glu_value, w_glu_gate, w_conv_gate,
-        w_beta, w_decay, decay_log, head_gain.reshape(1, 128), conv_taps,
+        w_beta.T, w_decay.T, decay_log, head_gain.reshape(1, 128), conv_taps,
         ln_gain.reshape(1, 128), ln_shift.reshape(1, 128), out_delta, out_conv,
     )
 

time: 95.2 us -> 70.3 us (0.74)
  Pallas kernels: 90.4 us -> 68.2 us
  local copies, waits for them, and re-layouts: 4.65 us -> 1.88 us
    pallas_call x1, Pallas kernels: 90.4 us -> 68.2 us  [local(): pl.pallas_call(kernel, out_shape=jax.ShapeDtypeStruct((BLK, 2048), BF), i...]
    unnamed x5 -> x1, local copies, waits for them, and re-layouts: 4.65 us -> 1.88 us
where the time goes in v2:
time: 70.3 us; the launch traced here: 70.1 us
  Pallas kernels  68.2 us (97%)
  local copies, waits for them, and re-layouts  1.88 us (3%)
    pallas_call x1, Pallas kernels, local(): pl.pallas_call(kernel, out_shape=jax.ShapeDtypeStruct((BLK, 2048), BF), i...  68.2 us
    unnamed x1, local copies, waits for them, and re-layouts  1.88 us

profile of v2, /device:TPU:1, one launch (start us, length us, event | category | flops | bytes accessed | tf_op | source)
XLA Modules:
  0.0 70.1 jit_solution(9284810706210447606)
XLA Ops:
  0.0 68.2 %layer.1 = bf16[128,2048]{1,0:T(8,128)(2,1)} custom-call(bf16[1024,256]{1,0:T(8,128)(2,1)} %x.1, bf16[2048,128]{1,0:T(8,128)(2,1)} %wq.1, bf16[2048,128]{1,0:T(8,128)(2,1)} %wk.1, bf16[2048,128]{1,0:T(8,128)(2,1)} %wv.1, bf16[2048,128]{1,0:T(8,128)(2,1)} %wdg.1, bf16[2048,128]{1,0:T(8,128)(2,1)} %wgv.1, bf16[2048,128]{1,0:T(8,128)(2,1)} %wgg.1, ...), custom_call_target="tpu_custom_call" | custom-call | tf_op jit(solution)/shard_map/layer/pallas_call | solution.py:510
  68.2 1.9 %copy.19 = bf16[128,2048]{1,0:T(8,128)(2,1)} copy(bf16[128,2048]{1,0:T(8,128)(2,1)} %layer.1) | data formatting | bytes 1048576

commit v3 on v2

--- a/solution.py
+++ b/solution.py
@@ -13,11 +13,15 @@
 CHUNK = 256
 CHUNKS = ROWS // CHUNK
 HALF = CHUNK // 2
-GROUP = 512
-PER = GROUP // BLK
 COLS = 8 * 128
-MOVES = 31
+SEMS = (
+    ("w", "wo", "x", "out", "gs", "ms", "xs", "zs", "fs", "hs", "ss", "ds", "cs")
+    + tuple(f"g{k}{r}" for k in range(3) for r in range(CHUNKS))
+    + ("a", "af", "by", "bf", "b0", "b1", "bx", "bm", "zy", "zf", "z0", "zx", "zm")
+    + ("xr", "zr", "fr", "hr", "sr", "dr", "cr")
+)
 TAPS = 31
+FAR_FIRST = (4, 5, 3, 2, 6, 1, 7)
 NORM = 1e-06
 VAR = 1e-05
 NN = ((1,), (0,))
@@ -65,8 +69,8 @@
     x, wq, wk, wv, wdg, wgv, wgg, wcg, wb, wd, dlog, hgain, taps, lng, lns, od, oc,
     out,
     xg, w, wo, qs, ks, vs, dgs, cgs, bes, lds, pad, filt, qcs, ocs, mn, mnx, mnz, s4s, s4r,
-    halo_s, halo_r, sts, str_, dms, cms, dmr, cmr, stage,
-    wsem, gs, gr, os_, or_, xs, xr, zs, zr, fs, fr, hs, hr, ss, sr, ds_, dr, cs, cr, osem,
+    halo_s, halo_r, sts, str_, dms, cms, dmr, cmr, stage, half,
+    sems,
 ):
     sp = lax.axis_index("sp")
     t = lax.axis_index("tp")
@@ -84,19 +88,25 @@
     def at_sp(k):
         return {"sp": k, "tp": t}
 
+    def sem(name):
+        return sems.at[SEMS.index(name)]
+
+    def await_bytes(ref, name):
+        pltpu.make_async_copy(ref, ref, sem(name)).wait()
+
     wrefs = (wq, wk, wv, wdg, wgv, wgg, wcg)
     wcopies = [
-        pltpu.make_async_copy(ref, w.at[:, k * 128 : (k + 1) * 128], wsem.at[k])
+        pltpu.make_async_copy(ref, w.at[:, k * 128 : (k + 1) * 128], sem("w"))
         for k, ref in enumerate(wrefs)
     ]
     own_rows = pl.ds(pl.multiple_of(t * 128, 128), 128)
-    wcopies.append(pltpu.make_async_copy(od, wo.at[0, own_rows, :], wsem.at[7]))
-    wcopies.append(pltpu.make_async_copy(oc, wo.at[1, own_rows, :], wsem.at[8]))
+    wcopies.append(pltpu.make_async_copy(od, wo.at[0, own_rows, :], sem("wo")))
+    wcopies.append(pltpu.make_async_copy(oc, wo.at[1, own_rows, :], sem("wo")))
 
     def cols_of(k):
         return pl.ds(pl.multiple_of(k * SHARD, SHARD), SHARD)
 
-    xcopy = pltpu.make_async_copy(x, xg.at[:, cols_of(t)], wsem.at[9])
+    xcopy = pltpu.make_async_copy(x, xg.at[:, cols_of(t)], sem("x"))
     xcopy.start()
     for cp in wcopies:
         cp.start()
@@ -105,7 +115,7 @@
     peers = [at_tp((t + d) % 8) for d in range(1, 8)]
     peers += [at_sp(z * 4 + (xx + d) % 4) for d in range(1, 4)]
     peers += [at_sp((zq * 4 + (zi + d) % 4) * 4 + xx) for d in range(1, 4)]
-    peers += [at_sp(((z + 4) % 8) * 4 + xx), at_sp((sp + 1) % 32), at_sp((sp + 31) % 32)]
+    peers += [at_sp((7 - z) * 4 + xx), at_sp((sp + 1) % 32), at_sp((sp + 31) % 32)]
     for peer in peers:
         pl.semaphore_signal(bar, inc=1, device_id=peer, device_id_type=pl.DeviceIdType.MESH)
     pl.semaphore_wait(bar, len(peers))
@@ -125,61 +135,91 @@
         shard = (t, t, t, left, right, left, right, opp, opp)[kind]
         to = (right, left, mate, right, left, mate, mate, mate, mate)[kind]
         dst = xg.at[rows, cols_of(shard)]
-        return send(dst, dst, gs.at[kind, r], gr.at[kind, r], at_tp(to))
+        return send(dst, dst, sem("gs"), sem(f"g{(0, 0, 2, 1, 1, 2, 2, 2, 2)[kind]}{r}"), at_tp(to))
 
     def own(r):
         for kind in (0, 1, 2):
             gat(kind, r).start()
 
     def relay1(r):
-        gat(0, r).wait_recv()
-        gat(3, r).start()
-        gat(5, r).start()
-        gat(1, r).wait_recv()
-        gat(4, r).start()
-        gat(6, r).start()
+        await_bytes(xg.at[0:CHUNK, 0:512], f"g0{r}")
+        for kind in (3, 4, 5, 6):
+            gat(kind, r).start()
 
     def relay2(r):
-        gat(3, r).wait_recv()
+        await_bytes(xg.at[0:CHUNK, 0:256], f"g1{r}")
         gat(7, r).start()
-        gat(4, r).wait_recv()
         gat(8, r).start()
 
     def rows_of(shard, off, n):
-        return pl.ds(pl.multiple_of(shard * 128 + off, 16), n)
+        return pl.ds(pl.multiple_of(shard * 128 + off, 8), n)
 
     near = (left, right, opp)
     xr_id = at_sp(z * 4 + (xx + 1) % 4)
     xl_id = at_sp(z * 4 + (xx + 3) % 4)
-    x_left, x_right, x_opp = (xx + 3) % 4, (xx + 1) % 4, (xx + 2) % 4
+    zr_id = at_sp(((z + 1) % 8) * 4 + xx)
+    zl_id = at_sp(((z + 7) % 8) * 4 + xx)
     moves = {"m": (wo.at[:, rows_of(t, 0, 128), :], at_tp(mate))}
-    for h in (0, 1):
-        a_own = wo.at[0, rows_of(t, 64 * h, 64), :]
-        moves["ar", h] = (a_own, at_tp(right))
-        moves["al", h] = (a_own, at_tp(left))
-        moves["afr", h] = (wo.at[0, rows_of(left, 64 * h, 32), :], at_tp(right))
-        moves["afl", h] = (wo.at[0, rows_of(right, 64 * h + 32, 32), :], at_tp(left))
+    a_own = wo.at[0, rows_of(t, 0, 64), :]
+    moves["ar"] = (a_own, at_tp(right))
+    moves["al"] = (a_own, at_tp(left))
+    moves["afr"] = (wo.at[0, rows_of(left, 0, 32), :], at_tp(right))
+    moves["afl"] = (wo.at[0, rows_of(right, 32, 32), :], at_tp(left))
     for j in range(3):
-        moves["am", j] = (wo.at[0, rows_of(near[j], 0, 128), :], at_tp(mate))
-    b_own = wo.at[1, rows_of(t, 32 * xx, 32), :]
-    moves["br"] = (b_own, at_tp(right))
-    moves["bl"] = (b_own, at_tp(left))
-    moves["bfr"] = (wo.at[1, rows_of(left, 32 * xx, 16), :], at_tp(right))
-    moves["bfl"] = (wo.at[1, rows_of(right, 32 * xx + 16, 16), :], at_tp(left))
-    for j in range(3):
-        b_mine = wo.at[1, rows_of(near[j], 32 * xx, 32), :]
-        moves["xr", j] = (b_mine, xr_id)
-        moves["xl", j] = (b_mine, xl_id)
-        moves["xfr", j] = (wo.at[1, rows_of(near[j], 32 * x_left, 16), :], xr_id)
-        moves["xfl", j] = (wo.at[1, rows_of(near[j], 32 * x_right + 16, 16), :], xl_id)
-        moves["xm", j] = (wo.at[1, rows_of(near[j], 0, 128), :], at_tp(mate))
-    assert len(moves) == MOVES
+        moves["am", j] = (wo.at[0, rows_of(near[j], 0, 64), :], at_tp(mate))
+
+    def spread_moves(name, w_at, base, piece, place, to_right, to_left):
+        def part(shard, off, n):
+            return wo.at[w_at, rows_of(shard, base + off, n), :]
+
+        half = piece // 2
+        mine = piece * place
+        before, after = piece * ((place + 3) % 4), piece * ((place + 1) % 4)
+        moves[name, "yr"] = (part(t, mine, piece), at_tp(right))
+        moves[name, "yl"] = (part(t, mine, piece), at_tp(left))
+        moves[name, "yfr"] = (part(left, mine, half), at_tp(right))
+        moves[name, "yfl"] = (part(right, mine + half, half), at_tp(left))
+        for j in range(3):
+            shard = near[j]
+            moves[name, "r", j] = (part(shard, mine, piece), to_right)
+            moves[name, "l", j] = (part(shard, mine, piece), to_left)
+            moves[name, "fr", j] = (part(shard, before, half), to_right)
+            moves[name, "fl", j] = (part(shard, after + half, half), to_left)
+            across = piece * ((place + 2) % 4)
+            for k, off in enumerate((mine, before, after, across)):
+                moves[name, f"m{k}", j] = (part(shard, off, piece), at_tp(mate))
+
+    spread_moves("b", 1, 0, 32, xx, xr_id, xl_id)
+    spread_moves("z", 0, 64, 16, zi, zr_id, zl_id)
+
+    def go(name, *tags):
+        for tag in tags:
+            for key in [k for k in moves if k[:2] == (name, tag)]:
+                move(*key).start()
+
+    def landing(key):
+        if key == "m":
+            return "bm"
+        if isinstance(key, str):
+            return "a" if key in ("ar", "al") else "af"
+        name, tag = key[:2]
+        if name == "am":
+            return "zm"
+        if tag in ("yr", "yl"):
+            return name + "y"
+        if tag in ("yfr", "yfl"):
+            return name + "f"
+        if tag in ("r", "l"):
+            return name + ("1" if name == "b" and key[2] > 0 else "0")
+        return name + ("x" if tag in ("fr", "fl") else "m")
 
     def move(*key):
         key = key if len(key) > 1 else key[0]
         ref, to = moves[key]
-        k = list(moves).index(key)
-        return send(ref, ref, os_.at[k], or_.at[k], to)
+        return send(ref, ref, sem("ms"), sem(landing(key)), to)
+
+    def got(name, rows):
+        await_bytes(wo.at[0, 0:rows, :], name)
 
     xcopy.wait()
     own(0)
@@ -199,11 +239,10 @@
     mn[:, :128] = (row == col).astype(F32)
     mn[:, 128:] = jnp.zeros((BLK, BLK), F32)
 
-    for cp in wcopies[:7]:
-        cp.wait()
+    await_bytes(w.at[:, :896], "w")
 
     def project(r):
-        rows = pl.ds(pl.multiple_of(r * CHUNK, CHUNK), CHUNK)
+        rows = slice(r * CHUNK, (r + 1) * CHUNK)
         xr_ = xg[rows, :]
         xf = xr_.astype(F32)
         inv = lax.rsqrt(jnp.sum(xf * xf, axis=1, keepdims=True) / 2048.0 + NORM)
@@ -221,11 +260,11 @@
         low_lanes = lax.broadcasted_iota(jnp.int32, (CHUNK, 128), 1) < 64
         bes[rows, :] = sigmoid(jnp.where(low_lanes, raw[7], turned))
         lds[rows, :] = -rate * softplus(jnp.where(low_lanes, turned, raw[7]))
-        below = pl.ds(pl.multiple_of(r * CHUNK + 32, 32), CHUNK)
+        below = slice(r * CHUNK + 32, (r + 1) * CHUNK + 32)
         pad[below, :] = (gv * sigmoid(gg)).astype(BF).astype(F32)
 
-    def delta(r):
-        spans = [pl.ds(pl.multiple_of(r * GROUP + b * BLK, BLK), BLK) for b in range(PER)]
+    def delta(first, last, mid=None):
+        spans = [slice(b * BLK, (b + 1) * BLK) for b in range(first, last)]
         sums, lows, scores = [], [], []
         for rows in spans:
             total = lax.dot_general(
@@ -240,6 +279,8 @@
             scores.append(both[BLK:] * damp)
             sums.append(total)
         inverses = block_inverse(lows)
+        if mid is not None:
+            mid()
         later = []
         for rows, total, score, inv in zip(spans, sums, scores, inverses):
             grow = jnp.exp(total)
@@ -266,66 +307,57 @@
         mn[...] = state
 
     def arrive(r):
-        for kind in (2, 5, 6, 7, 8):
-            gat(kind, r).wait_recv()
+        await_bytes(xg.at[0:CHUNK, 0:1024], f"g2{r}")
 
     relay1(0)
     own(2)
     relay1(1)
     own(3)
     relay2(0)
-    for kk in (7, 8):
-        wcopies[kk].wait()
-
-    @pl.loop(0, 2)
-    def _(p):
-        arrive(2 * p)
-        project(2 * p)
-
-        @pl.when(p == 0)
-        def _():
-            relay1(2)
-            relay2(1)
-
-        arrive(2 * p + 1)
-        project(2 * p + 1)
-
-        @pl.when(p == 0)
-        def _():
-            relay1(3)
-
-        delta(p)
-
-        @pl.when(p == 0)
-        def _():
-            relay2(2)
-            relay2(3)
-            for key in ("br", "bl", "m"):
-                move(key).start()
-            move("ar", 0).start()
-            move("al", 0).start()
-
+    await_bytes(wo.at[:, 0:128, :], "wo")
+
+    arrive(0)
+    project(0)
+    relay1(2)
+    delta(0, 2, lambda: relay2(1))
+    relay1(3)
+    arrive(1)
+    project(1)
+
+    def middle():
+        relay2(2)
+        go("b", "yr", "yl")
+        go("z", "yr", "yl")
+
+    delta(2, 4, middle)
+    relay2(3)
+    move("m").start()
+    arrive(2)
+    project(2)
+    arrive(3)
+    project(3)
+    delta(4, 8)
     own_x = mn[...].astype(BF)
     mnx[xx] = own_x
 
     def xsend(d):
-        return send(mnx.at[xx], mnx.at[xx], xs.at[d - 1], xr.at[d - 1],
+        return send(mnx.at[xx], mnx.at[xx], sem("xs"), sem("xr"),
                     at_sp(z * 4 + (xx + d) % 4))
 
     for d in (1, 2, 3):
         xsend(d).start()
     halo_s[...] = pad[ROWS : ROWS + 32, :].astype(BF)
-    hcopy = send(halo_s, halo_r, hs, hr, at_sp((sp + 1) % 32))
+    hcopy = send(halo_s, halo_r, sem("hs"), sem("hr"), at_sp((sp + 1) % 32))
     hcopy.start()
-    move("br").wait_recv()
-    move("bfr").start()
-    move("bl").wait_recv()
-    move("bfl").start()
-    move("ar", 1).start()
-    move("al", 1).start()
-    for j in (0, 1):
-        move("xr", j).start()
-        move("xl", j).start()
+    for name, rows in (("b", 64), ("z", 32)):
+        got(name + "y", rows)
+        go(name, "yfr", "yfl")
+        for j in (0, 1):
+            move(name, "r", j).start()
+            move(name, "l", j).start()
+            move(name, "m0", j).start()
+    move("ar").start()
+    move("al").start()
 
     tapf = taps[...].astype(F32)
 
@@ -350,7 +382,7 @@
         sts[1:2, lanes] = jnp.sum(ft * ft, axis=0, keepdims=True)
 
     def ssend(d):
-        return send(sts, str_.at[t], ss.at[d - 1], sr.at[d - 1], at_tp((t + d) % 8))
+        return send(sts, str_.at[t], sem("ss"), sem("sr"), at_tp((t + d) % 8))
 
     for d in range(1, 8):
         ssend(d).start()
@@ -371,29 +403,26 @@
                 n_in = jnp.where(mine > k, total[:, 128:], n_in)
         return m_in, n_in, total
 
-    for d in (1, 2, 3):
-        xsend(d).wait_recv()
+    await_bytes(mnx.at[0:3], "xr")
     mxp, nxp, xtotal = chain(mnx, xx)
     mnz[zi] = xtotal.astype(BF)
 
     def zsend(d):
-        return send(mnz.at[zi], mnz.at[zi], zs.at[d - 1], zr.at[d - 1],
+        return send(mnz.at[zi], mnz.at[zi], sem("zs"), sem("zr"),
                     at_sp((zq * 4 + (zi + d) % 4) * 4 + xx))
 
     for d in (1, 2, 3):
         zsend(d).start()
 
-    move("bfr").wait_recv()
-    move("bfl").wait_recv()
-    move("xr", 2).start()
-    move("xl", 2).start()
-    move("ar", 0).wait_recv()
-    move("afr", 0).start()
-    move("al", 0).wait_recv()
-    move("afl", 0).start()
-
-    for d in range(1, 8):
-        ssend(d).wait_recv()
+    got("bf", 32)
+    got("zf", 16)
+    for name in ("b", "z"):
+        for tag in ("r", "l", "m0"):
+            move(name, tag, 2).start()
+    got("b0", 64)
+    for tag in ("fr", "fl", "m1", "m2"):
+        move("b", tag, 0).start()
+    await_bytes(str_.at[0:7], "sr")
     both = str_[0]
     for k in range(1, 8):
         both = both + str_[k]
@@ -410,92 +439,85 @@
     def a2a(src, dst, s_sem, r_sem, d):
         to = (t + d) % 8
         rows = pl.ds(pl.multiple_of(to * BLK, BLK), BLK)
-        return send(src.at[rows, :], dst.at[t], s_sem.at[d - 1], r_sem.at[d - 1], at_tp(to))
-
-    for d in range(1, 8):
-        a2a(cms, cmr, cs, cr, d).start()
+        return send(src.at[rows, :], dst.at[t], sem(s_sem), sem(r_sem), at_tp(to))
+
+    for d in FAR_FIRST:
+        a2a(cms, cmr, "cs", "cr", d).start()
     cmr[t] = cms[own_rows, :]
-
-    for d in (1, 2, 3):
-        zsend(d).wait_recv()
+    got("a", 128)
+    for key in ("afr", "afl"):
+        move(key).start()
+    move("am", 0).start()
+    move("am", 1).start()
+
+    await_bytes(mnz.at[0:3], "zr")
     mzp, nzp, ztotal = chain(mnz, zi)
     s4s[...] = ztotal[:, 128:].astype(BF)
-    fcopy = send(s4s, s4r, fs, fr, at_sp(((z + 4) % 8) * 4 + xx))
+    fcopy = send(s4s, s4r, sem("fs"), sem("fr"), at_sp((7 - z) * 4 + xx))
     fcopy.start()
     moved = mm(mxp, jnp.concatenate([mzp, nzp], axis=1))
     mpre, npre = moved[:, :128], moved[:, 128:] + nxp
-    for j in (0, 1, 2):
-        move("xr", j).wait_recv()
-        move("xfr", j).start()
-        move("xl", j).wait_recv()
-        move("xfl", j).start()
-    move("ar", 1).wait_recv()
-    move("afr", 1).start()
-    move("am", 0).start()
-    move("al", 1).wait_recv()
-    move("afl", 1).start()
-    move("am", 1).start()
+    got("b1", 128)
+    for j in (1, 2):
+        for tag in ("fr", "fl", "m1", "m2"):
+            move("b", tag, j).start()
+    got("z0", 96)
+    go("z", "fr", "fl", "m1", "m2")
     fcopy.wait_recv()
     begin = s4r[...].astype(F32) * (zq > 0).astype(F32)
     carried = mm(mpre, begin) + npre
 
-    for b in range(ROWS // BLK):
-        lanes = slice(b * BLK, (b + 1) * BLK)
+    for i, d in enumerate(FAR_FIRST + (0,)):
+        lanes = pl.ds(pl.multiple_of(lax.rem(t + d, 8) * BLK, BLK), BLK)
         o = ocs[lanes, :] + mm(qcs[lanes, :], carried)
         o = o * lax.rsqrt(jnp.mean(o * o, axis=-1, keepdims=True) + NORM) * hgain[...]
         dms[lanes, :] = (o * dgs[lanes, :]).astype(BF)
-    for d in range(1, 8):
-        a2a(dms, dmr, ds_, dr, d).start()
+        if i in (3, 7):
+            for e in FAR_FIRST[max(i - 4, 0) : i]:
+                a2a(dms, dmr, "ds", "dr", e).start()
     dmr[t] = dms[own_rows, :]
 
-    for j in (0, 1, 2):
-        move("xfr", j).wait_recv()
-        move("xfl", j).wait_recv()
-        move("xm", j).start()
-    for h in (0, 1):
-        move("afr", h).wait_recv()
-        move("afl", h).wait_recv()
+    got("bx", 96)
+    go("b", "m3")
+    got("zx", 48)
+    go("z", "m3")
+    got("af", 64)
     move("am", 2).start()
-    for d in range(1, 8):
-        a2a(cms, cmr, cs, cr, d).wait_recv()
-    move("m").wait_recv()
-    for j in (0, 1, 2):
-        move("xm", j).wait_recv()
-        move("am", j).wait_recv()
-    for d in range(1, 8):
-        a2a(dms, dmr, ds_, dr, d).wait_recv()
+    await_bytes(cmr.at[0:7], "cr")
+    got("bm", 640)
+    lhs_c = jnp.concatenate([cmr[k] for k in range(8)], axis=1)
+
+    @pl.loop(0, 8)
+    def _(n):
+        lanes = pl.ds(pl.multiple_of(n * 256, 256), 256)
+        half[n] = jnp.dot(lhs_c, wo[1, :, lanes], preferred_element_type=F32)
+
+    got("zm", 384)
+    await_bytes(dmr.at[0:7], "dr")
 
     lhs_d = jnp.concatenate([dmr[k] for k in range(8)], axis=1)
-    lhs_c = jnp.concatenate([cmr[k] for k in range(8)], axis=1)
 
     def ocopy(n):
         lanes = pl.ds(pl.multiple_of(n * 256, 256), 256)
-        return pltpu.make_async_copy(stage.at[n], out.at[:, lanes], osem.at[n])
+        return pltpu.make_async_copy(stage.at[n], out.at[:, lanes], sem("out"))
 
     @pl.loop(0, 8)
     def _(n):
         lanes = pl.ds(pl.multiple_of(n * 256, 256), 256)
         acc = jnp.dot(lhs_d, wo[0, :, lanes], preferred_element_type=F32)
-        acc = acc + jnp.dot(lhs_c, wo[1, :, lanes], preferred_element_type=F32)
-        stage[n] = acc.astype(BF)
+        stage[n] = (acc + half[n]).astype(BF)
         ocopy(n).start()
 
-    for n in range(8):
-        ocopy(n).wait()
-    for r in range(CHUNKS):
-        for kind in range(9):
-            gat(kind, r).wait_send()
-    for key in moves:
-        move(*(key if isinstance(key, tuple) else (key,))).wait_send()
-    for d in (1, 2, 3):
-        xsend(d).wait_send()
-        zsend(d).wait_send()
-    hcopy.wait_send()
-    fcopy.wait_send()
-    for d in range(1, 8):
-        ssend(d).wait_send()
-        a2a(cms, cmr, cs, cr, d).wait_send()
-        a2a(dms, dmr, ds_, dr, d).wait_send()
+    await_bytes(stage, "out")
+    await_bytes(xg.at[0:896, :], "gs")
+    await_bytes(wo.at[:, 0:896, :], "ms")
+    await_bytes(mnx.at[0:3], "xs")
+    await_bytes(mnz.at[0:3], "zs")
+    await_bytes(s4s, "fs")
+    await_bytes(halo_s, "hs")
+    await_bytes(str_.at[0:7], "ss")
+    await_bytes(dmr.at[0:7], "ds")
+    await_bytes(cmr.at[0:7], "cs")
 
 
 def local(*args):
@@ -532,12 +554,8 @@
             pltpu.VMEM((8, BLK, BLK), BF),
             pltpu.VMEM((8, BLK, BLK), BF),
             pltpu.VMEM((8, BLK, 256), BF),
-            dma((10,)),
-            dma((9, CHUNKS)), dma((9, CHUNKS)),
-            dma((MOVES,)), dma((MOVES,)),
-            dma((3,)), dma((3,)), dma((3,)), dma((3,)),
-            dma, dma, dma, dma,
-            dma((7,)), dma((7,)), dma((7,)), dma((7,)), dma((7,)), dma((7,)), dma((8,)),
+            pltpu.VMEM((8, BLK, 256), F32),
+            dma((len(SEMS),)),
         ],
         compiler_params=pltpu.CompilerParams(
             collective_id=0, has_side_effects=True, vmem_limit_bytes=60 * 1024 * 1024

time: 70.3 us -> 65.7 us (0.935)
  Pallas kernels: 68.2 us -> 63.6 us
    pallas_call x1, Pallas kernels: 68.2 us -> 63.6 us  [local(): pl.pallas_call(kernel, out_shape=jax.ShapeDtypeStruct((BLK, 2048), BF), i...]
where the time goes in v3:
time: 65.7 us; the launch traced here: 65.5 us
  Pallas kernels  63.6 us (97%)
  local copies, waits for them, and re-layouts  1.88 us (3%)
    pallas_call x1, Pallas kernels, local(): pl.pallas_call(kernel, out_shape=jax.ShapeDtypeStruct((BLK, 2048), BF), i...  63.6 us
    unnamed x1, local copies, waits for them, and re-layouts  1.88 us

profile of v3, /device:TPU:1, one launch (start us, length us, event | category | flops | bytes accessed | tf_op | source)
XLA Modules:
  0.0 65.5 jit_solution(9119769630426931018)
XLA Ops:
  0.0 63.6 %layer.1 = bf16[128,2048]{1,0:T(8,128)(2,1)} custom-call(bf16[1024,256]{1,0:T(8,128)(2,1)} %x.1, bf16[2048,128]{1,0:T(8,128)(2,1)} %wq.1, bf16[2048,128]{1,0:T(8,128)(2,1)} %wk.1, bf16[2048,128]{1,0:T(8,128)(2,1)} %wv.1, bf16[2048,128]{1,0:T(8,128)(2,1)} %wdg.1, bf16[2048,128]{1,0:T(8,128)(2,1)} %wgv.1, bf16[2048,128]{1,0:T(8,128)(2,1)} %wgg.1, ...), custom_call_target="tpu_custom_call" | custom-call | tf_op jit(solution)/shard_map/layer/pallas_call | solution.py:532
  63.6 1.9 %copy.19 = bf16[128,2048]{1,0:T(8,128)(2,1)} copy(bf16[128,2048]{1,0:T(8,128)(2,1)} %layer.1) | data formatting | bytes 1048576

commit v4 on v3

--- a/solution.py
+++ b/solution.py
@@ -15,10 +15,10 @@
 HALF = CHUNK // 2
 COLS = 8 * 128
 SEMS = (
-    ("w", "wo", "x", "out", "gs", "ms", "xs", "zs", "fs", "hs", "ss", "ds", "cs")
+    ("w", "wo", "x", "out", "gs", "ms", "xs", "zs1", "zs2", "zs3", "fs", "hs", "ss", "ds", "cs")
     + tuple(f"g{k}{r}" for k in range(3) for r in range(CHUNKS))
     + ("a", "af", "by", "bf", "b0", "b1", "bx", "bm", "zy", "zf", "z0", "zx", "zm")
-    + ("xr", "zr", "fr", "hr", "sr", "dr", "cr")
+    + ("xr", "zr1", "zr2", "zr3", "fr", "hr", "sr", "dr", "cr")
 )
 TAPS = 31
 FAR_FIRST = (4, 5, 3, 2, 6, 1, 7)
@@ -70,7 +70,7 @@
     out,
     xg, w, wo, qs, ks, vs, dgs, cgs, bes, lds, pad, filt, qcs, ocs, mn, mnx, mnz, s4s, s4r,
     halo_s, halo_r, sts, str_, dms, cms, dmr, cmr, stage, half,
-    sems,
+    sems, ack,
 ):
     sp = lax.axis_index("sp")
     t = lax.axis_index("tp")
@@ -111,14 +111,43 @@
     for cp in wcopies:
         cp.start()
 
+    mnz[...] = jnp.zeros(mnz.shape, BF)
+    s4r[...] = jnp.zeros(s4r.shape, BF)
+    halo_r[...] = jnp.zeros(halo_r.shape, BF)
     bar = pltpu.get_barrier_semaphore()
-    peers = [at_tp((t + d) % 8) for d in range(1, 8)]
-    peers += [at_sp(z * 4 + (xx + d) % 4) for d in range(1, 4)]
-    peers += [at_sp((zq * 4 + (zi + d) % 4) * 4 + xx) for d in range(1, 4)]
-    peers += [at_sp((7 - z) * 4 + xx), at_sp((sp + 1) % 32), at_sp((sp + 31) % 32)]
-    for peer in peers:
-        pl.semaphore_signal(bar, inc=1, device_id=peer, device_id_type=pl.DeviceIdType.MESH)
-    pl.semaphore_wait(bar, len(peers))
+
+    def signal(semaphore, peer):
+        pl.semaphore_signal(
+            semaphore, inc=1, device_id=peer, device_id_type=pl.DeviceIdType.MESH
+        )
+
+    def signal_if(condition, semaphore, peer):
+        @pl.when(condition)
+        def _():
+            signal(semaphore, peer)
+
+    for d in range(1, 8):
+        signal(bar, at_tp((t + d) % 8))
+    for d in range(1, 4):
+        signal(bar, at_sp(z * 4 + (xx + d) % 4))
+    for d in range(1, 4):
+        signal_if(zi + d < 4, bar, at_sp((sp + 4 * d) % 32))
+    for d in range(1, 5):
+        signal_if(z == 3, bar, at_sp((sp + 4 * d) % 32))
+    signal_if(z < 7, bar, at_sp((sp + 4) % 32))
+    signal_if(z == 0, bar, at_sp((sp + 28) % 32))
+    signal_if((xx == 3) & (z < 7), bar, at_sp((sp + 1) % 32))
+
+    def count(*conditions):
+        return sum(jnp.where(condition, 1, 0) for condition in conditions)
+
+    pl.semaphore_wait(bar, 10 + zi + count(z >= 4, z > 0, z == 7, (xx == 0) & (z > 0)))
+    for d in range(1, 4):
+        signal_if(zi - d >= 0, ack, at_sp((sp + 32 - 4 * d) % 32))
+    signal_if(z >= 4, ack, at_sp(12 + xx))
+    signal_if(z > 0, ack, at_sp((sp + 28) % 32))
+    signal_if(z == 7, ack, at_sp((sp + 4) % 32))
+    signal_if((xx == 0) & (z > 0), ack, at_sp((sp + 31) % 32))
 
     def send(src, dst, ssem, rsem, to):
         return pltpu.make_async_remote_copy(
@@ -348,7 +377,17 @@
         xsend(d).start()
     halo_s[...] = pad[ROWS : ROWS + 32, :].astype(BF)
     hcopy = send(halo_s, halo_r, sem("hs"), sem("hr"), at_sp((sp + 1) % 32))
-    hcopy.start()
+
+    @pl.when(z < 7)
+    def _():
+        pl.semaphore_wait(
+            ack, 3 - zi + 1 + count(z == 0, xx == 3) + 4 * count(z == 3)
+        )
+
+    @pl.when(sp < 31)
+    def _():
+        hcopy.start()
+
     for name, rows in (("b", 64), ("z", 32)):
         got(name + "y", rows)
         go(name, "yfr", "yfl")
@@ -371,7 +410,10 @@
     def _(i):
         conv_rows(i)
 
-    hcopy.wait_recv()
+    @pl.when(sp > 0)
+    def _():
+        hcopy.wait_recv()
+
     keep = (sp > 0).astype(F32)
     pad[0:32, :] = halo_r[...].astype(F32) * keep
     conv_rows(0)
@@ -408,11 +450,15 @@
     mnz[zi] = xtotal.astype(BF)
 
     def zsend(d):
-        return send(mnz.at[zi], mnz.at[zi], sem("zs"), sem("zr"),
-                    at_sp((zq * 4 + (zi + d) % 4) * 4 + xx))
+        return send(mnz.at[zi], mnz.at[zi], sem(f"zs{d}"), sem(f"zr{d}"), at_sp((sp + 4 * d) % 32))
+
+    def upward(d, act):
+        @pl.when(zi + d < 4)
+        def _():
+            act(zsend(d))
 
     for d in (1, 2, 3):
-        zsend(d).start()
+        upward(d, lambda copy: copy.start())
 
     got("bf", 32)
     got("zf", 16)
@@ -450,11 +496,22 @@
     move("am", 0).start()
     move("am", 1).start()
 
-    await_bytes(mnz.at[0:3], "zr")
+    for d in (1, 2, 3):
+        @pl.when(zi - d >= 0)
+        def _():
+            zsend(d).wait_recv()
+
     mzp, nzp, ztotal = chain(mnz, zi)
     s4s[...] = ztotal[:, 128:].astype(BF)
-    fcopy = send(s4s, s4r, sem("fs"), sem("fr"), at_sp((7 - z) * 4 + xx))
-    fcopy.start()
+
+    def fcopy(d):
+        return send(s4s, s4r, sem("fs"), sem("fr"), at_sp((sp + 4 * d) % 32))
+
+    @pl.when(z == 3)
+    def _():
+        for d in (4, 3, 2, 1):
+            fcopy(d).start()
+
     moved = mm(mxp, jnp.concatenate([mzp, nzp], axis=1))
     mpre, npre = moved[:, :128], moved[:, 128:] + nxp
     got("b1", 128)
@@ -463,7 +520,10 @@
             move("b", tag, j).start()
     got("z0", 96)
     go("z", "fr", "fl", "m1", "m2")
-    fcopy.wait_recv()
+    @pl.when(z >= 4)
+    def _():
+        fcopy(1).wait_recv()
+
     begin = s4r[...].astype(F32) * (zq > 0).astype(F32)
     carried = mm(mpre, begin) + npre
 
@@ -512,9 +572,18 @@
     await_bytes(xg.at[0:896, :], "gs")
     await_bytes(wo.at[:, 0:896, :], "ms")
     await_bytes(mnx.at[0:3], "xs")
-    await_bytes(mnz.at[0:3], "zs")
-    await_bytes(s4s, "fs")
-    await_bytes(halo_s, "hs")
+    for d in (1, 2, 3):
+        upward(d, lambda copy: copy.wait_send())
+
+    @pl.when(z == 3)
+    def _():
+        await_bytes(mnx.at[0:2], "fs")
+
+
+    @pl.when(sp < 31)
+    def _():
+        await_bytes(halo_s, "hs")
+
     await_bytes(str_.at[0:7], "ss")
     await_bytes(dmr.at[0:7], "ds")
     await_bytes(cmr.at[0:7], "cs")
@@ -556,6 +625,7 @@
             pltpu.VMEM((8, BLK, 256), BF),
             pltpu.VMEM((8, BLK, 256), F32),
             dma((len(SEMS),)),
+            pltpu.SemaphoreType.REGULAR,
         ],
         compiler_params=pltpu.CompilerParams(
             collective_id=0, has_side_effects=True, vmem_limit_bytes=60 * 1024 * 1024

time: 65.7 us -> 63.8 us (0.971)
  Pallas kernels: 63.6 us -> 61.7 us
    pallas_call x1, Pallas kernels: 63.6 us -> 61.7 us  [local(): pl.pallas_call(kernel, out_shape=jax.ShapeDtypeStruct((BLK, 2048), BF), i...]
where the time goes in v4:
time: 63.8 us; the launch traced here: 63.6 us
  Pallas kernels  61.7 us (97%)
  local copies, waits for them, and re-layouts  1.88 us (3%)
    pallas_call x1, Pallas kernels, local(): pl.pallas_call(kernel, out_shape=jax.ShapeDtypeStruct((BLK, 2048), BF), i...  61.7 us
    unnamed x1, local copies, waits for them, and re-layouts  1.88 us

profile of v4, /device:TPU:1, one launch (start us, length us, event | category | flops | bytes accessed | tf_op | source)
XLA Modules:
  0.0 63.6 jit_solution(18242772800175892162)
XLA Ops:
  0.0 61.7 %layer.1 = bf16[128,2048]{1,0:T(8,128)(2,1)} custom-call(bf16[1024,256]{1,0:T(8,128)(2,1)} %x.1, bf16[2048,128]{1,0:T(8,128)(2,1)} %wq.1, bf16[2048,128]{1,0:T(8,128)(2,1)} %wk.1, bf16[2048,128]{1,0:T(8,128)(2,1)} %wv.1, bf16[2048,128]{1,0:T(8,128)(2,1)} %wdg.1, bf16[2048,128]{1,0:T(8,128)(2,1)} %wgv.1, bf16[2048,128]{1,0:T(8,128)(2,1)} %wgg.1, ...), custom_call_target="tpu_custom_call" | custom-call | tf_op jit(solution)/shard_map/layer/pallas_call | solution.py:601
  61.8 1.9 %copy.19 = bf16[128,2048]{1,0:T(8,128)(2,1)} copy(bf16[128,2048]{1,0:T(8,128)(2,1)} %layer.1) | data formatting | bytes 1048576

commit v5 on v4

--- a/solution.py
+++ b/solution.py
@@ -395,8 +395,6 @@
             move(name, "r", j).start()
             move(name, "l", j).start()
             move(name, "m0", j).start()
-    move("ar").start()
-    move("al").start()
 
     tapf = taps[...].astype(F32)
 
@@ -410,6 +408,8 @@
     def _(i):
         conv_rows(i)
 
+    move("ar").start()
+    move("al").start()
     @pl.when(sp > 0)
     def _():
         hcopy.wait_recv()
@@ -445,6 +445,9 @@
                 n_in = jnp.where(mine > k, total[:, 128:], n_in)
         return m_in, n_in, total
 
+    got("zf", 16)
+    for tag in ("r", "l", "m0"):
+        move("z", tag, 2).start()
     await_bytes(mnx.at[0:3], "xr")
     mxp, nxp, xtotal = chain(mnx, xx)
     mnz[zi] = xtotal.astype(BF)
@@ -461,10 +464,8 @@
         upward(d, lambda copy: copy.start())
 
     got("bf", 32)
-    got("zf", 16)
-    for name in ("b", "z"):
-        for tag in ("r", "l", "m0"):
-            move(name, tag, 2).start()
+    for tag in ("r", "l", "m0"):
+        move("b", tag, 2).start()
     got("b0", 64)
     for tag in ("fr", "fl", "m1", "m2"):
         move("b", tag, 0).start()
@@ -539,18 +540,25 @@
 
     got("bx", 96)
     go("b", "m3")
-    got("zx", 48)
-    go("z", "m3")
-    got("af", 64)
-    move("am", 2).start()
     await_bytes(cmr.at[0:7], "cr")
     got("bm", 640)
     lhs_c = jnp.concatenate([cmr[k] for k in range(8)], axis=1)
 
-    @pl.loop(0, 8)
-    def _(n):
+    def conv_part(n):
         lanes = pl.ds(pl.multiple_of(n * 256, 256), 256)
         half[n] = jnp.dot(lhs_c, wo[1, :, lanes], preferred_element_type=F32)
+
+    @pl.loop(0, 4)
+    def _(n):
+        conv_part(n)
+
+    got("af", 64)
+    move("am", 2).start()
+    got("zx", 48)
+    go("z", "m3")
+    @pl.loop(4, 8)
+    def _(n):
+        conv_part(n)
 
     got("zm", 384)
     await_bytes(dmr.at[0:7], "dr")

time: 63.8 us -> 63.5 us (level)
  no operation moved by 1% of the time
where the time goes in v5:
time: 63.5 us; the launch traced here: 63.3 us
  Pallas kernels  61.4 us (97%)
  local copies, waits for them, and re-layouts  1.88 us (3%)
    pallas_call x1, Pallas kernels, local(): pl.pallas_call(kernel, out_shape=jax.ShapeDtypeStruct((BLK, 2048), BF), i...  61.4 us
    unnamed x1, local copies, waits for them, and re-layouts  1.88 us

profile of v5, /device:TPU:1, one launch (start us, length us, event | category | flops | bytes accessed | tf_op | source)
XLA Modules:
  0.0 63.3 jit_solution(12910192252576453335)
XLA Ops:
  0.0 61.4 %layer.1 = bf16[128,2048]{1,0:T(8,128)(2,1)} custom-call(bf16[1024,256]{1,0:T(8,128)(2,1)} %x.1, bf16[2048,128]{1,0:T(8,128)(2,1)} %wq.1, bf16[2048,128]{1,0:T(8,128)(2,1)} %wk.1, bf16[2048,128]{1,0:T(8,128)(2,1)} %wv.1, bf16[2048,128]{1,0:T(8,128)(2,1)} %wdg.1, bf16[2048,128]{1,0:T(8,128)(2,1)} %wgv.1, bf16[2048,128]{1,0:T(8,128)(2,1)} %wgg.1, ...), custom_call_target="tpu_custom_call" | custom-call | tf_op jit(solution)/shard_map/layer/pallas_call | solution.py:609
  61.4 1.9 %copy.19 = bf16[128,2048]{1,0:T(8,128)(2,1)} copy(bf16[128,2048]{1,0:T(8,128)(2,1)} %layer.1) | data formatting | bytes 1048576

commit v6 on v5

--- a/solution.py
+++ b/solution.py
@@ -408,8 +408,6 @@
     def _(i):
         conv_rows(i)
 
-    move("ar").start()
-    move("al").start()
     @pl.when(sp > 0)
     def _():
         hcopy.wait_recv()
@@ -466,6 +464,8 @@
     got("bf", 32)
     for tag in ("r", "l", "m0"):
         move("b", tag, 2).start()
+    move("ar").start()
+    move("al").start()
     got("b0", 64)
     for tag in ("fr", "fl", "m1", "m2"):
         move("b", tag, 0).start()
@@ -491,11 +491,6 @@
     for d in FAR_FIRST:
         a2a(cms, cmr, "cs", "cr", d).start()
     cmr[t] = cms[own_rows, :]
-    got("a", 128)
-    for key in ("afr", "afl"):
-        move(key).start()
-    move("am", 0).start()
-    move("am", 1).start()
 
     for d in (1, 2, 3):
         @pl.when(zi - d >= 0)
@@ -521,6 +516,11 @@
             move("b", tag, j).start()
     got("z0", 96)
     go("z", "fr", "fl", "m1", "m2")
+    got("a", 128)
+    for key in ("afr", "afl"):
+        move(key).start()
+    move("am", 0).start()
+    move("am", 1).start()
     @pl.when(z >= 4)
     def _():
         fcopy(1).wait_recv()

time: 63.5 us -> 63.5 us (level)
  no operation moved by 1% of the time
where the time goes in v6:
time: 63.5 us; the launch traced here: 63.3 us
  Pallas kernels  61.4 us (97%)
  local copies, waits for them, and re-layouts  1.88 us (3%)
    pallas_call x1, Pallas kernels, local(): pl.pallas_call(kernel, out_shape=jax.ShapeDtypeStruct((BLK, 2048), BF), i...  61.4 us
    unnamed x1, local copies, waits for them, and re-layouts  1.88 us

profile of v6, /device:TPU:1, one launch (start us, length us, event | category | flops | bytes accessed | tf_op | source)
XLA Modules:
  0.0 63.3 jit_solution(8238488763454161984)
XLA Ops:
  0.0 61.4 %layer.1 = bf16[128,2048]{1,0:T(8,128)(2,1)} custom-call(bf16[1024,256]{1,0:T(8,128)(2,1)} %x.1, bf16[2048,128]{1,0:T(8,128)(2,1)} %wq.1, bf16[2048,128]{1,0:T(8,128)(2,1)} %wk.1, bf16[2048,128]{1,0:T(8,128)(2,1)} %wv.1, bf16[2048,128]{1,0:T(8,128)(2,1)} %wdg.1, bf16[2048,128]{1,0:T(8,128)(2,1)} %wgv.1, bf16[2048,128]{1,0:T(8,128)(2,1)} %wgg.1, ...), custom_call_target="tpu_custom_call" | custom-call | tf_op jit(solution)/shard_map/layer/pallas_call | solution.py:609
  61.4 1.9 %copy.19 = bf16[128,2048]{1,0:T(8,128)(2,1)} copy(bf16[128,2048]{1,0:T(8,128)(2,1)} %layer.1) | data formatting | bytes 1048576

commit v7 on v6

--- a/solution.py
+++ b/solution.py
@@ -296,10 +296,13 @@
         spans = [slice(b * BLK, (b + 1) * BLK) for b in range(first, last)]
         sums, lows, scores = [], [], []
         for rows in spans:
-            total = lax.dot_general(
-                tri, lds[rows, :], (NN, ((), ())),
-                precision=lax.Precision.HIGHEST, preferred_element_type=F32,
-            )
+            log = lds[rows, :]
+            top = log.astype(BF)
+            rest = log - top.astype(F32)
+            middle = rest.astype(BF)
+            least = (rest - middle.astype(F32)).astype(BF)
+            terms = mm(tri, jnp.concatenate([top, middle, least], axis=1))
+            total = terms[:, :128] + (terms[:, 128:256] + terms[:, 256:])
             spread = total - total.T
             damp = jnp.where(causal, jnp.exp(jnp.where(causal, spread, 0.0)), 0.0)
             kb = ks[rows, :].astype(BF)

time: 63.5 us -> 63.4 us (level)
  no operation moved by 1% of the time
where the time goes in v7:
time: 63.4 us; the launch traced here: 63.3 us
  Pallas kernels  61.4 us (97%)
  local copies, waits for them, and re-layouts  1.88 us (3%)
    pallas_call x1, Pallas kernels, local(): pl.pallas_call(kernel, out_shape=jax.ShapeDtypeStruct((BLK, 2048), BF), i...  61.4 us
    unnamed x1, local copies, waits for them, and re-layouts  1.88 us

profile of v7, /device:TPU:1, one launch (start us, length us, event | category | flops | bytes accessed | tf_op | source)
XLA Modules:
  0.0 63.3 jit_solution(8816588285961769612)
XLA Ops:
  0.0 61.4 %layer.1 = bf16[128,2048]{1,0:T(8,128)(2,1)} custom-call(bf16[1024,256]{1,0:T(8,128)(2,1)} %x.1, bf16[2048,128]{1,0:T(8,128)(2,1)} %wq.1, bf16[2048,128]{1,0:T(8,128)(2,1)} %wk.1, bf16[2048,128]{1,0:T(8,128)(2,1)} %wv.1, bf16[2048,128]{1,0:T(8,128)(2,1)} %wdg.1, bf16[2048,128]{1,0:T(8,128)(2,1)} %wgv.1, bf16[2048,128]{1,0:T(8,128)(2,1)} %wgg.1, ...), custom_call_target="tpu_custom_call" | custom-call | tf_op jit(solution)/shard_map/layer/pallas_call | solution.py:612
  61.4 1.9 %copy.19 = bf16[128,2048]{1,0:T(8,128)(2,1)} copy(bf16[128,2048]{1,0:T(8,128)(2,1)} %layer.1) | data formatting | bytes 1048576
